TPU v7x, 32 devices: a whole 2x2x4 slice. The times are simulated.
32 devices in a mesh: sp: 8 (over z, x), tp: 4 (over y, core).
Axes of the slice: x: 2, y: 2, z: 4, core: 2. Of those that a mesh axis runs over, the one named last changes fastest.
Arguments:
- layer_input: bfloat16 [1024, 2048], P('sp'), may hold values from -6 to 6
- out_cot: bfloat16 [1024, 2048], P('sp'), may hold values from -6 to 6
- routes: int32 [1024, 2], P('sp'), may hold values from 0 to 7, all different within a row; in each aligned block of 128 rows (0 to 127, 128 to 255, ...) at most 64 rows name the same one
- route_weights: float32 [1024, 2], P('sp'), may hold values from 0.2 to 1
- gate_weights: bfloat16 [8, 2048, 1024], P('sp', None, 'tp'), may hold values from -0.125 to 0.125
- up_weights: bfloat16 [8, 2048, 1024], P('sp', None, 'tp'), may hold values from -0.125 to 0.125
- down_weights: bfloat16 [8, 1024, 2048], P('sp', 'tp'), may hold values from -0.1875 to 0.1875
- out_proj: bfloat16 [2048, 2048], P(None, 'tp'), may hold values from -0.125 to 0.125
- queries: bfloat16 [1024, 2048], P('sp', 'tp'), may hold values from -6 to 6
- keys: bfloat16 [1024, 2048], P('sp', 'tp'), may hold values from -6 to 6
- values: bfloat16 [1024, 2048], P('sp', 'tp'), may hold values from -6 to 6
- mixer_out: bfloat16 [1024, 2048], P('sp', 'tp'), may hold values from -6 to 6
- entry_states: float32 [8, 32, 64, 64], P('sp', 'tp'), may hold values from -6 to 6
Outputs:
- grad_gate: bfloat16 [8, 2048, 1024], P('sp', None, 'tp')
- grad_up: bfloat16 [8, 2048, 1024], P('sp', None, 'tp')
- grad_down: bfloat16 [8, 1024, 2048], P('sp', 'tp')
- grad_proj: float32 [2048, 2048], P('sp', 'tp')
- grad_queries: bfloat16 [1024, 2048], P('sp', 'tp')
- grad_keys: bfloat16 [1024, 2048], P('sp', 'tp')
- grad_values: bfloat16 [1024, 2048], P('sp', 'tp')
Inputs may be any that keep to these rules, and one draw needn't show every extreme that they name: `routes`: in each aligned block of 128 rows no expert is named by more than 64 rows, a bound that some block reaches; the numbers of one row differ.
All inputs are finite; a program needn't handle non-finite values.
Results may differ from a plain program's by a relative error of at most 0.01.
Values may be sent and summed in bfloat16 or wider, within the bound.
No kernel may reach another device: no remote copies, remote signals or barrier semaphores. Data moves between devices by JAX's collectives and lax.ppermute only.
A program may use at most 128 MiB of HBM per device.

v0:
```python
import jax
import jax.numpy as jnp
from jax import lax
from jax.sharding import PartitionSpec as P

DK = 64
SPAN = 128


def prefix(array, axis, combine, identity):
    devices, position = (lax.axis_size(axis), lax.axis_index(axis))
    everything = jax.tree.map(lambda part: lax.all_gather(part, axis), array)
    start = jax.tree.map(
        lambda part, zero: jnp.broadcast_to(jnp.asarray(zero, part.dtype), part.shape),
        array,
        identity,
    )

    def hop(k, before):
        at = devices - 1 - k
        reached = at > position
        new = combine(before, jax.tree.map(lambda part: part[at], everything))
        return jax.tree.map(lambda a, b: jnp.where(reached, a, b), new, before)

    return lax.fori_loop(0, devices, hop, start)


def decay_rates(head_ids, head_count, token_count):
    half_count = head_count // 2
    fraction = jnp.minimum(head_ids, half_count) / half_count
    base_rate = jnp.exp(
        (1.0 - fraction) * jnp.log(1.0 / 32.0) + fraction * jnp.log(1.0 / token_count)
    )
    return base_rate * (1.0 + jnp.maximum(head_ids - half_count, 0.0) / half_count)


def position_norm(positions, head_rates):
    return jnp.sqrt(
        jnp.expm1(-2.0 * head_rates)[None, :]
        / jnp.expm1(-2.0 * head_rates[None, :] * (positions[:, None] + 1.0))
    )


def expert_grads(exp_rows, exp_cot, activated, d_gate, d_up):
    row_dims = (((0,), (0,)), ((), ()))
    grad_gate = lax.dot_general(
        exp_rows, d_gate, row_dims, preferred_element_type=jnp.float32
    ).astype(jnp.bfloat16)
    grad_up = lax.dot_general(exp_rows, d_up, row_dims, preferred_element_type=jnp.float32).astype(
        jnp.bfloat16
    )
    grad_down = lax.dot_general(
        activated, exp_cot, row_dims, preferred_element_type=jnp.float32
    ).astype(jnp.bfloat16)
    return (grad_gate[None], grad_up[None], grad_down[None])


def later_first(earlier, later):
    return (earlier[0] * later[0], later[1] + later[0][:, None, None] * earlier[1])


def per_device(
    layer_input,
    out_cot,
    routes,
    route_weights,
    gate_weights,
    up_weights,
    down_weights,
    out_proj,
    queries,
    keys,
    values,
    mixer_out,
    entry_states,
):
    tok_rows, model_width = layer_input.shape
    experts = lax.axis_size("sp")
    narrow = lax.axis_size("tp")
    top_count = routes.shape[1]
    pair_count = tok_rows * top_count
    capacity = 2 * pair_count // experts
    flat_routes = routes.reshape(pair_count)
    onehot = (flat_routes[:, None] == jnp.arange(experts, dtype=jnp.int32)[None, :]).astype(
        jnp.int32
    )
    earlier = jnp.cumsum(onehot, axis=0) - onehot
    target = flat_routes * capacity + jnp.sum(earlier * onehot, axis=1)
    owner_tok = jnp.arange(pair_count, dtype=jnp.int32) // top_count
    slot_tok = jnp.full((experts * capacity,), tok_rows, jnp.int32).at[target].set(owner_tok)
    slot_weight = (
        jnp.zeros((experts * capacity,), jnp.float32)
        .at[target]
        .set(route_weights.reshape(pair_count))
    )
    blank_row = jnp.zeros((1, model_width), jnp.bfloat16)
    sent_rows = jnp.concatenate([layer_input, blank_row], 0)[slot_tok].reshape(
        experts, capacity, model_width
    )
    picked_cot = jnp.concatenate([out_cot, blank_row], 0)[slot_tok]
    sent_cot = (
        (slot_weight[:, None] * picked_cot.astype(jnp.float32))
        .astype(jnp.bfloat16)
        .reshape(experts, capacity, model_width)
    )
    share = capacity // narrow
    first_row = lax.axis_index("tp") * share
    part_rows = lax.dynamic_slice_in_dim(sent_rows, first_row, share, 1)
    part_cot = lax.dynamic_slice_in_dim(sent_cot, first_row, share, 1)
    got_rows, got_cot = (
        lax.all_to_all(part_rows, "sp", split_axis=0, concat_axis=0, tiled=True),
        lax.all_to_all(part_cot, "sp", split_axis=0, concat_axis=0, tiled=True),
    )
    got_rows, got_cot = (
        lax.all_gather(got_rows, "tp", axis=1, tiled=True),
        lax.all_gather(got_cot, "tp", axis=1, tiled=True),
    )
    exp_rows = got_rows.reshape(experts * capacity, model_width)
    exp_cot = got_cot.reshape(experts * capacity, model_width)
    gate_w = gate_weights[0]
    up_w = up_weights[0]
    down_w = down_weights[0]
    gate_pre = jnp.dot(exp_rows, gate_w, preferred_element_type=jnp.float32)
    up_pre = jnp.dot(exp_rows, up_w, preferred_element_type=jnp.float32)
    sigmoid_g = jax.nn.sigmoid(gate_pre)
    activated = (gate_pre * sigmoid_g * up_pre).astype(jnp.bfloat16)
    width_dims = (((1,), (1,)), ((), ()))
    d_act = lax.dot_general(exp_cot, down_w, width_dims, preferred_element_type=jnp.float32)
    d_gate = (d_act * up_pre * sigmoid_g * (1.0 + gate_pre * (1.0 - sigmoid_g))).astype(
        jnp.bfloat16
    )
    d_up = (d_act * gate_pre * sigmoid_g).astype(jnp.bfloat16)
    grads = expert_grads(exp_rows, exp_cot, activated, d_gate, d_up)
    partial_sum = lax.dot_general(d_gate, gate_w, width_dims, preferred_element_type=jnp.float32)
    partial_sum = partial_sum + lax.dot_general(
        d_up, up_w, width_dims, preferred_element_type=jnp.float32
    )
    summed = lax.psum_scatter(
        partial_sum.reshape(experts, capacity, model_width), "tp", scatter_dimension=2, tiled=True
    )
    returned = lax.all_to_all(
        summed.astype(jnp.bfloat16), "sp", split_axis=0, concat_axis=0, tiled=True
    )
    col_count = model_width // narrow
    first_col = lax.axis_index("tp") * col_count
    back_flat = returned.reshape(experts * capacity, col_count)
    pair_back = back_flat[target].reshape(tok_rows, top_count, col_count).astype(jnp.float32)
    own_cols = lax.dynamic_slice_in_dim(out_cot, first_col, col_count, 1).astype(jnp.float32)
    cot_cols = (own_cols + jnp.sum(pair_back, axis=1)).astype(jnp.bfloat16)
    mixer_cot = lax.all_gather(cot_cols, "tp", axis=1, tiled=True)
    grad_proj = lax.psum_scatter(
        lax.dot_general(
            mixer_cot, mixer_out, (((0,), (0,)), ((), ())), preferred_element_type=jnp.float32
        ),
        "sp",
        scatter_dimension=0,
        tiled=True,
    )
    head_count = queries.shape[1] // DK
    head_ids = (lax.axis_index("tp") * head_count + jnp.arange(head_count, dtype=jnp.int32)).astype(
        jnp.float32
    )
    head_rates = decay_rates(head_ids, head_count * narrow, tok_rows * experts)
    positions = (lax.axis_index("sp") * tok_rows + jnp.arange(tok_rows, dtype=jnp.int32)).astype(
        jnp.float32
    )
    head_cot = jnp.dot(mixer_cot, out_proj, preferred_element_type=jnp.float32).reshape(
        tok_rows, head_count, DK
    )
    head_cot = (head_cot * position_norm(positions, head_rates)[:, :, None]).astype(jnp.bfloat16)
    span_count = tok_rows // SPAN
    span_shape = (span_count, SPAN, head_count, DK)
    span_query = queries.reshape(span_shape)
    span_key = keys.reshape(span_shape)
    span_value = values.reshape(span_shape)
    span_cot = head_cot.reshape(span_shape)
    key_scale = DK ** (-0.5)
    offsets = jnp.arange(SPAN, dtype=jnp.float32)
    distance = offsets[:, None] - offsets[None, :]
    decay_mat = jnp.where(
        distance[None] >= 0,
        jnp.exp(-head_rates[:, None, None] * jnp.maximum(distance, 0.0)[None]),
        0.0,
    )
    fwd_weights = (
        jnp.einsum("cihd,cjhd->chij", span_query, span_key, preferred_element_type=jnp.float32)
        * key_scale
        * decay_mat[None]
    ).astype(jnp.bfloat16)
    back_weights = (
        jnp.einsum("cihd,cjhd->chij", span_cot, span_value, preferred_element_type=jnp.float32)
        * decay_mat[None]
    ).astype(jnp.bfloat16)
    tail_decay = jnp.exp(-head_rates[None, :] * (SPAN - 1.0 - offsets)[:, None])
    lead_decay = jnp.exp(-head_rates[None, :] * (offsets + 1.0)[:, None])
    span_decay = jnp.exp(-head_rates * SPAN)
    query_wide = span_query.astype(jnp.float32)
    key_wide = span_key.astype(jnp.float32)
    value_wide = span_value.astype(jnp.float32)
    cot_wide = span_cot.astype(jnp.float32)
    updates = key_scale * jnp.einsum(
        "cjhd,cjhe->chde",
        key_wide * tail_decay[None, :, :, None],
        value_wide,
        precision=lax.Precision.HIGHEST,
    )
    backs = jnp.einsum(
        "cihd,cihe->chde",
        query_wide * lead_decay[None, :, :, None],
        cot_wide,
        precision=lax.Precision.HIGHEST,
    )
    carried = entry_states[0]
    span_id = 0
    fwd_states = [carried]
    carried = span_decay[:, None, None] * carried + updates[span_id]
    reverse_state = jnp.zeros_like(carried)
    rev_local = [reverse_state] * span_count
    span_id = 0
    rev_local[span_id] = reverse_state
    reverse_state = span_decay[:, None, None] * reverse_state + backs[span_id]
    dev_decay = jnp.exp(-head_rates * tok_rows)
    identity = (jnp.ones_like(dev_decay), jnp.zeros_like(reverse_state))
    from_later = prefix((dev_decay, reverse_state), "sp", later_first, identity)[1]
    rev_states = jnp.stack(
        [
            rev_local[0]
            + jnp.exp(-head_rates * ((span_count - 1) * SPAN))[:, None, None] * from_later
        ]
    )
    fwd_stack = jnp.stack(fwd_states)
    grad_q = key_scale * jnp.einsum(
        "chij,cjhd->cihd", back_weights, span_key, preferred_element_type=jnp.float32
    )
    grad_q = grad_q + lead_decay[None, :, :, None] * jnp.einsum(
        "chde,cihe->cihd", fwd_stack, cot_wide, precision=lax.Precision.HIGHEST
    )
    grad_k = jnp.einsum(
        "chij,cihd->cjhd", back_weights, span_query, preferred_element_type=jnp.float32
    )
    grad_k = key_scale * (
        grad_k
        + tail_decay[None, :, :, None]
        * jnp.einsum("chde,cjhe->cjhd", rev_states, value_wide, precision=lax.Precision.HIGHEST)
    )
    grad_v = jnp.einsum(
        "chij,cihe->cjhe", fwd_weights, span_cot, preferred_element_type=jnp.float32
    )
    grad_v = grad_v + key_scale * tail_decay[None, :, :, None] * jnp.einsum(
        "chde,cjhd->cjhe", rev_states, key_wide, precision=lax.Precision.HIGHEST
    )
    flat_shape = (tok_rows, head_count * DK)
    return (
        grads[0],
        grads[1],
        grads[2],
        grad_proj,
        grad_q.reshape(flat_shape).astype(jnp.bfloat16),
        grad_k.reshape(flat_shape).astype(jnp.bfloat16),
        grad_v.reshape(flat_shape).astype(jnp.bfloat16),
    )


def solution(mesh):
    placed = (
        P("sp", None),
        P("sp", None),
        P("sp", None),
        P("sp", None),
        P("sp", None, "tp"),
        P("sp", None, "tp"),
        P("sp", "tp", None),
        P(None, "tp"),
        P("sp", "tp"),
        P("sp", "tp"),
        P("sp", "tp"),
        P("sp", "tp"),
        P("sp", "tp", None, None),
    )
    return jax.shard_map(
        per_device,
        mesh=mesh,
        in_specs=placed,
        out_specs=(
            P("sp", None, "tp"),
            P("sp", None, "tp"),
            P("sp", "tp", None),
            P("sp", "tp"),
            P("sp", "tp"),
            P("sp", "tp"),
            P("sp", "tp"),
        ),
        check_vma=False,
    )
```

profile of v0, /device:TPU:0, one launch (start us, length us, event | category | flops | bytes accessed | tf_op | source)
XLA Modules:
  0.0 315.5 jit_solution(11229628259408267841)
XLA Ops:
  10.3 1.4 scatter_custom_fusion
  12.9 3.3 %gather_fusion = bf16[512,2048]{1,0:T(8,128)(2,1)} fusion(bf16[129,2048]{1,0:T(8,128)(2,1)S(1)} %concatenate.6, s32[1024]{0:T(1024)S(1)} %pad_clamp_fusion.1), kind=kCustom, calls=%fused_computation | custom fusion | bytes 4196352 | tf_op jit(solution)/shard_map/gather | solution.py:97
  17.3 21.7 %all_to_all.15 = bf16[8,16,2048]{2,1,0:T(8,128)(2,1)} all-to-all(bf16[8,16,2048]{2,1,0:T(8,128)(2,1)S(1)} %constant_dynamic-slice_fusion.1), channel_id=1, replica_groups=mesh['sp'=8,'tp'=4] {'sp'}, dimensions={0} | all-to-all | bytes 1048576 | tf_op jit(solution)/shard_map/all_to_all | solution.py:111
  39.4 1.4 scatter_custom_fusion.1
  40.9 3.3 %gather_fusion.1 = bf16[512,2048]{1,0:T(8,128)(2,1)} fusion(bf16[129,2048]{1,0:T(8,128)(2,1)S(1)} %concatenate.7, s32[1024]{0:T(1024)S(1)} %pad_clamp_fusion.1), kind=kCustom, calls=%fused_computation.1 | custom fusion | bytes 4196352 | tf_op jit(solution)/shard_map/gather | solution.py:100
  45.5 17.6 %all_to_all.16 = bf16[8,16,2048]{2,1,0:T(8,128)(2,1)} all-to-all(bf16[8,16,2048]{2,1,0:T(8,128)(2,1)S(1)} %fusion.18), channel_id=1, replica_groups=mesh['sp'=8,'tp'=4] {'sp'}, dimensions={0} | all-to-all | bytes 1048576 | tf_op jit(solution)/shard_map/all_to_all | solution.py:112
  63.2 3.5 %fusion.21 = f32[512,256]{1,0:T(8,128)} fusion(bf16[512,2048]{1,0:T(8,128)(2,1)} %bitcast.165, bf16[1,2048,256]{2,1,0:T(8,128)(2,1)} %param.19), kind=kOutput, calls=%fused_computation.42 | convolution fusion | flops 536870912 | bytes 3670016 | tf_op jit(solution)/shard_map/dot_general | solution.py:123
  66.8 1.5 fusion.24
  68.3 16.7 %all-gather.8.cloned.1.call-done = bf16[8,64,2048]{2,1,0:T(8,128)(2,1)} async-done(((bf16[8,16,2048]{2,1,0:T(8,128)(2,1)}), bf16[8,64,2048]{2,1,0:T(8,128)(2,1)}) %all-gather.8.cloned.1.call-update) | async-done | bytes 2097168 | tf_op jit(solution)/shard_map/all_gather | solution.py:116
  85.0 3.0 multiply_convert_fusion.1
  88.8 2.8 convolution_add_fusion
  91.6 44.6 %reduce-scatter.3.cloned.1.call-done = f32[8,64,512]{2,1,0:T(8,128)} async-done(((f32[8,64,2048]{2,1,0:T(8,128)}), f32[8,64,512]{2,1,0:T(8,128)}) %reduce-scatter.3.cloned.1.call-update) | async-done | bytes 1048592 | tf_op jit(solution)/shard_map/reduce_scatter | solution.py:138
  136.2 2.1 convert_element_type.144
  138.3 5.5 %all-to-all-start.2 = ((bf16[8,64,512]{2,1,0:T(8,128)(2,1)}), bf16[8,64,512]{2,1,0:T(8,128)(2,1)S(1)}, u32[]{:S(2)}, u32[]{:S(2)}) async-start(bf16[8,64,512]{2,1,0:T(8,128)(2,1)} %convert_element_type.144), calls=%async_computation.3 | async-start | bytes 1048576 | tf_op jit(solution)/shard_map/all_to_all | solution.py:141
  144.2 13.9 %all-to-all-done.2 = bf16[8,64,512]{2,1,0:T(8,128)(2,1)S(1)} async-done(((bf16[8,64,512]{2,1,0:T(8,128)(2,1)}), bf16[8,64,512]{2,1,0:T(8,128)(2,1)S(1)}, u32[]{:S(2)}, u32[]{:S(2)}) %all-to-all-start.2) | async-done | bytes 524320 | tf_op jit(solution)/shard_map/all_to_all | solution.py:141
  161.2 6.7 %all_gather.19 = bf16[128,2048]{1,0:T(8,128)(2,1)S(1)} all-gather(bf16[128,512]{1,0:T(8,128)(2,1)S(1)} %add_convert_fusion), channel_id=1, replica_groups=mesh['sp'=8,'tp'=4] {'tp'}, dimensions={1}, use_global_device_ids=true | all-gather | bytes 655360 | tf_op jit(solution)/shard_map/all_gather | solution.py:150
  169.9 2.7 fusion.56
  173.8 19.2 %all-gather.1 = f32[8,1,8]{2,1,0:T(1,128)S(1)} all-gather(f32[1,1,8]{2,1,0:T(1,128)S(1)} %exponential_bitcast_fusion), channel_id=1, replica_groups=mesh['sp'=8,'tp'=4] {'sp'}, dimensions={0}, use_global_device_ids=true | all-gather | bytes 288 | tf_op jit(solution)/shard_map/all_gather | solution.py:12
  193.1 3.5 %fusion.1 = bf16[1,2048,256]{2,1,0:T(8,128)(2,1)} fusion(bf16[512,2048]{1,0:T(8,128)(2,1)} %bitcast.166, bf16[512,256]{1,0:T(8,128)(2,1)S(1)} %copy-done.9), kind=kOutput, calls=%fused_computation.12 | convolution fusion | flops 537395200 | bytes 3407872 | tf_op jit(solution)/shard_map/dot_general | solution.py:46
  196.6 1.8 fusion.2
  198.7 1.8 fusion.3
  202.1 15.9 %all-gather.10.cloned.1.call-done = f32[64,64,64]{2,1,0:T(8,128)} async-done(((f32[8,64,64]{2,1,0:T(8,128)}), f32[64,64,64]{2,1,0:T(8,128)}) %all-gather.10.cloned.1.call-update) | async-done | bytes 1048592 | tf_op jit(solution)/shard_map/all_gather | solution.py:12
  218.0 8.8 %while.16 = (s32[]{:T(128)}, f32[8,64,64]{2,1,0:T(8,128)S(1)}, s32[]{:T(128)}, f32[8,8,64,64]{3,2,1,0:T(8,128)}, f32[8,8]{1,0:T(8,128)S(1)}, /*index=5*/s32[]{:T(128)}, s32[]{:T(128)}, s32[]{:T(128)}, s32[]{:T(128)}) while((s32[]{:T(128)}, f32[8,64,64]{2,1,0:T(8,128)S(1)}, s32[]{:T(128)}, f32[8,8,64,64]{3,2,1,0:T(8,128)}, ...), condition=%wide.region_9.10_spmd.clone, body=%wide.region_8.9_spmd.clone.sunk | while | flops 131080 | bytes 393487 | solution.py:25
  229.8 79.2 %reduce-scatter.5.cloned.1.call-done = f32[256,512]{1,0:T(8,128)} async-done(((f32[2048,512]{1,0:T(8,128)}), f32[256,512]{1,0:T(8,128)}) %reduce-scatter.5.cloned.1.call-update) | async-done | bytes 524304 | tf_op jit(solution)/shard_map/reduce_scatter | solution.py:151
  (118 shorter events, 28.1 us)
Async XLA Ops:
  7.2 160.7 %copy-start = (bf16[2048,512]{1,0:T(8,128)(2,1)S(1)}, bf16[2048,512]{1,0:T(8,128)(2,1)}, u32[]{:S(2)}) copy-start(bf16[2048,512]{1,0:T(8,128)(2,1)} %param.22) | copy-start | bytes 6291460
  7.2 56.0 %all-gather.6.cloned.1.call-start = ((), (), s32[]{:S(2)}) async-start(), calls=%async_computation.5 | async-start | bytes 2621440 | tf_op jit(solution)/shard_map/all_gather | solution.py:115
  16.2 22.9 %copy-start.14 = (f32[128,2]{0,1:T(2,128)S(1)}, f32[128,2]{0,1:T(2,128)}, u32[]{:S(2)}) copy-start(f32[128,2]{0,1:T(2,128)} %param.18) | copy-start | bytes 3076
  16.2 24.7 %copy-start.4 = (bf16[128,2048]{1,0:T(8,128)(2,1)S(1)}, bf16[128,2048]{1,0:T(8,128)(2,1)}, u32[]{:S(2)}) copy-start(bf16[128,2048]{1,0:T(8,128)(2,1)} %param.16) | copy-start | bytes 1572868
  39.1 45.9 %all-gather.8.cloned.1.call-start = ((), (), s32[]{:S(2)}) async-start(), calls=%async_computation.6 | async-start | bytes 2621440 | tf_op jit(solution)/shard_map/all_gather | solution.py:116
  63.1 3.6 %copy-start.2 = (bf16[1,2048,256]{2,1,0:T(8,128)(2,1)S(1)}, bf16[1,2048,256]{2,1,0:T(8,128)(2,1)}, u32[]{:S(2)}) copy-start(bf16[1,2048,256]{2,1,0:T(8,128)(2,1)} %param.20) | copy-start | bytes 3145732
  63.2 73.0 %reduce-scatter.3.cloned.1.call-start = ((), (), s32[]{:S(2)}) async-start(), calls=%async_computation.7 | async-start | bytes 5242880 | tf_op jit(solution)/shard_map/reduce_scatter | solution.py:138
  63.2 3.5 %copy-start.15 = (bf16[8,64,2048]{2,1,0:T(8,128)(2,1)S(1)}, bf16[8,64,2048]{2,1,0:T(8,128)(2,1)}, u32[]{:S(2)}) copy-start(bf16[8,64,2048]{2,1,0:T(8,128)(2,1)} %all-gather.6.cloned.1.call-done) | copy-start | bytes 6291460
  85.0 3.1 copy-start.3
  88.0 0.8 copy-start.8
  91.6 52.2 %copy-start.11 = (bf16[128,512]{1,0:T(8,128)(2,1)S(1)}, bf16[128,512]{1,0:T(8,128)(2,1)}, u32[]{:S(2)}) copy-start(bf16[128,512]{1,0:T(8,128)(2,1)} %param.23) | copy-start | bytes 393220
  138.3 19.8 %all-to-all-start.2 = ((bf16[8,64,512]{2,1,0:T(8,128)(2,1)}), bf16[8,64,512]{2,1,0:T(8,128)(2,1)S(1)}, u32[]{:S(2)}, u32[]{:S(2)}) async-start(bf16[8,64,512]{2,1,0:T(8,128)(2,1)} %convert_element_type.144), calls=%async_computation.3 | async-start | bytes 1048576 | tf_op jit(solution)/shard_map/all_to_all | solution.py:141
  143.8 74.2 %all-gather.10.cloned.1.call-start = ((), (), s32[]{:S(2)}) async-start(), calls=%async_computation.9 | async-start | bytes 2359296 | tf_op jit(solution)/shard_map/all_gather | solution.py:12
  167.8 2.1 copy-start.10
  169.9 139.1 %reduce-scatter.5.cloned.1.call-start = ((), (), s32[]{:S(2)}) async-start(), calls=%async_computation.8 | async-start | bytes 4718592 | tf_op jit(solution)/shard_map/reduce_scatter | solution.py:151
  172.6 0.9 copy-start.12
  172.6 1.0 copy-start.13
  172.6 20.5 %copy-start.9 = (bf16[512,256]{1,0:T(8,128)(2,1)S(1)}, bf16[512,256]{1,0:T(8,128)(2,1)}, u32[]{:S(2)}) copy-start(bf16[512,256]{1,0:T(8,128)(2,1)} %copy-done.8) | copy-start | bytes 786436
  193.1 3.5 %copy-start.16 = (bf16[8,64,2048]{2,1,0:T(8,128)(2,1)S(1)}, bf16[8,64,2048]{2,1,0:T(8,128)(2,1)}, u32[]{:S(2)}) copy-start(bf16[8,64,2048]{2,1,0:T(8,128)(2,1)} %all-gather.6.cloned.1.call-done) | copy-start | bytes 6291460
  196.6 1.8 copy-start.1
  196.6 1.8 copy-start.5
  196.6 2.2 copy-start.6
  198.7 2.3 copy-start.7
Sparse Core Ops, SparseCore 0:
  39.2 21.5 all-gather.5
  63.3 21.6 all-gather.7
  91.7 44.4 reduce-scatter.2
  170.0 47.9 all-gather.9
  222.0 86.8 reduce-scatter.4
where the time goes:
time: 316 us; the launch traced here: 315 us
  waiting for transfers between devices  170 us (54%)
  blocking collectives  65.2 us (21%)
  matrix products  25.4 us (8%)
  local copies, waits for them, and re-layouts  19.2 us (6%)
  other arithmetic  15.2 us (5%)
  between operations  14.2 us (4%)
  starting transfers between devices  5.69 us (2%)
    reduce_scatter x1, waiting for transfers between devices, per_device(): lax.psum_scatter(lax.dot_general(mixer_cot, mixer_out, (((0,), (0,)), (()...  79.2 us
    reduce_scatter x1, waiting for transfers between devices, per_device(): lax.psum_scatter(partial_sum.reshape(experts, capacity, model_width), 'tp...  44.6 us
    all_to_all x1, blocking collectives, per_device(): lax.all_to_all(part_rows, 'sp', split_axis=0, concat_axis=0, tiled=True)  21.7 us
    all_gather x1, blocking collectives, prefix(): everything = jax.tree.map(lambda part: lax.all_gather(part, axis), array)  19.2 us
    all_to_all x1, blocking collectives, per_device(): lax.all_to_all(part_cot, 'sp', split_axis=0, concat_axis=0, tiled=True)  17.6 us
    all_gather x1, waiting for transfers between devices, per_device(): lax.all_gather(got_cot, 'tp', axis=1, tiled=True)  16.7 us
    all_gather x1, waiting for transfers between devices, prefix(): everything = jax.tree.map(lambda part: lax.all_gather(part, axis), array)  15.9 us
    all_to_all x1, waiting for transfers between devices, per_device(): lax.all_to_all(summed.astype(jnp.bfloat16), 'sp', split_axis=0, concat_ax...  13.9 us
  transfers between devices with their start and end apart: 6, of which 5 were waited for; matrix products, arithmetic and copies ran while one was open for 11% of the time, Pallas kernels for 0%

commit v1 on v0

v1 whole, which is shorter than its diff:
```python
import functools

import jax
import jax.numpy as jnp
from jax import lax
from jax.experimental import pallas as pl
from jax.experimental.pallas import tpu as pltpu
from jax.sharding import PartitionSpec as P

DK = 64
SPAN = 128
F32 = jnp.float32
BF16 = jnp.bfloat16
NN = (((1,), (0,)), ((), ()))
NT = (((1,), (1,)), ((), ()))
TN = (((0,), (0,)), ((), ()))


def dot(a, b, dims=NN, precision=None):
    return lax.dot_general(a, b, dims, precision=precision, preferred_element_type=F32)


def decay_rates(head_ids, head_count, token_count):
    half_count = head_count // 2
    fraction = jnp.minimum(head_ids, half_count) / half_count
    base_rate = jnp.exp(
        (1.0 - fraction) * jnp.log(1.0 / 32.0) + fraction * jnp.log(1.0 / token_count)
    )
    return base_rate * (1.0 + jnp.maximum(head_ids - half_count, 0.0) / half_count)


def position_norm(positions, head_rates):
    return jnp.sqrt(
        jnp.expm1(-2.0 * head_rates)[None, :]
        / jnp.expm1(-2.0 * head_rates[None, :] * (positions[:, None] + 1.0))
    )


def slot_table(routes, experts):
    tokens = routes.shape[0]
    lanes = lax.broadcasted_iota(jnp.int32, (tokens, experts), 1)
    named = jnp.zeros((tokens, experts), F32)
    for k in range(routes.shape[1]):
        named = named + (routes[:, k : k + 1] == lanes).astype(F32)
    row = lax.broadcasted_iota(jnp.int32, (tokens, tokens), 0)
    col = lax.broadcasted_iota(jnp.int32, (tokens, tokens), 1)
    before = (col < row).astype(BF16)
    earlier = dot(before, named.astype(BF16))
    return named * (earlier + 1.0), lanes


def dispatch_kernel(me_ref, routes_ref, weights_ref, rows_ref, cot_ref, out_rows, out_cot, *, experts, share):
    routes = routes_ref[...]
    table, lanes = slot_table(routes, experts)
    picks = experts * share
    tokens = routes.shape[0]
    owner = lax.broadcasted_iota(jnp.int32, (picks, experts), 0) // share
    of_expert = owner == lax.broadcasted_iota(jnp.int32, (picks, experts), 1)
    spread = dot(of_expert.astype(BF16), table.astype(BF16), NT)
    wanted = lax.broadcasted_iota(jnp.int32, (picks, tokens), 0) % share + me_ref[0] * share + 1
    chosen = spread == wanted.astype(F32)
    pick = chosen.astype(BF16)
    weight = jnp.zeros((tokens, experts), F32)
    for k in range(routes.shape[1]):
        weight = weight + jnp.where(routes[:, k : k + 1] == lanes, weights_ref[:, k : k + 1], 0.0)
    slot_weight = jnp.sum(
        jnp.where(of_expert, dot(chosen.astype(F32), weight, precision=lax.Precision.HIGHEST), 0.0),
        axis=1,
        keepdims=True,
    )
    out_rows[...] = dot(pick, rows_ref[...]).astype(BF16)
    out_cot[...] = (slot_weight * dot(pick, cot_ref[...])).astype(BF16)


def combine_kernel(me_ref, routes_ref, cot_ref, back_ref, out_ref, *, experts, share, masks):
    table, _ = slot_table(routes_ref[...], experts)
    capacity = share * len(masks)
    picks = experts * capacity
    place = lax.broadcasted_iota(jnp.int32, (picks, experts), 0)
    of_expert = (place // capacity == lax.broadcasted_iota(jnp.int32, (picks, experts), 1)).astype(BF16)
    spread = dot(table.astype(BF16), of_expert, NT)
    at = lax.broadcasted_iota(jnp.int32, spread.shape, 1) % capacity
    part = at // share
    mask = jnp.zeros_like(part)
    for p, m in enumerate(masks):
        mask = jnp.where(part == p, m, mask)
    wanted = (mask ^ me_ref[0]) * share + at % share + 1
    pick = (spread == wanted.astype(F32)).astype(BF16)
    out_ref[...] = (cot_ref[...].astype(F32) + dot(pick, back_ref[...])).astype(BF16)


def hidden_kernel(*refs, parts):
    row_refs, (gate_ref, up_ref, act_ref, fac_gate, fac_up) = refs[:parts], refs[parts:]
    for p, row_ref in enumerate(row_refs):
        rows = row_ref[...]
        gate_pre = dot(rows, gate_ref[...])
        up_pre = dot(rows, up_ref[...])
        sig = jax.nn.sigmoid(gate_pre)
        silu = gate_pre * sig
        act_ref[p] = (silu * up_pre).astype(BF16)
        fac_gate[p] = up_pre * sig * (1.0 + gate_pre * (1.0 - sig))
        fac_up[p] = silu


def back_kernel(me_ref, *refs, parts, orders):
    cot_refs = refs[:parts]
    down_ref, fac_gate, fac_up, gate_ref, up_ref, dgate_ref, dup_ref = refs[parts : parts + 7]
    outs = refs[parts + 7 :]
    width = gate_ref.shape[0]
    cols = width // parts
    grads = []
    for p in range(parts):
        d_act = dot(cot_refs[p][...], down_ref[...], NT)
        d_gate = (d_act * fac_gate[p]).astype(BF16)
        d_up = (d_act * fac_up[p]).astype(BF16)
        dgate_ref[p] = d_gate
        dup_ref[p] = d_up
        grads.append((d_gate, d_up))
    for out, (mask, order) in zip(outs, orders):
        first = pl.multiple_of((me_ref[0] ^ mask) * cols, cols)
        gate = gate_ref[pl.ds(first, cols), :]
        up = up_ref[pl.ds(first, cols), :]
        for p in range(parts):
            value = dot(grads[p][0], gate, NT) + dot(grads[p][1], up, NT)
            out[order[p]] = value.astype(out.dtype)


def vmem():
    return pl.BlockSpec(memory_space=pltpu.VMEM)


def smem():
    return pl.BlockSpec(memory_space=pltpu.SMEM)


def cost(flops, nbytes):
    return pl.CostEstimate(flops=int(flops), bytes_accessed=int(nbytes), transcendentals=0)


def per_device(
    layer_input,
    out_cot,
    routes,
    route_weights,
    gate_weights,
    up_weights,
    down_weights,
    out_proj,
    queries,
    keys,
    values,
    mixer_out,
    entry_states,
):
    tok_rows, width = layer_input.shape
    experts = lax.axis_size("sp")
    narrow = lax.axis_size("tp")
    here = lax.axis_index("sp")
    me = lax.axis_index("tp")
    me_arr = me.astype(jnp.int32).reshape(1)
    capacity = 2 * tok_rows * routes.shape[1] // experts
    share = capacity // narrow
    picks = experts * share
    cols = width // narrow
    gate_w, up_w, down_w = gate_weights[0], up_weights[0], down_weights[0]
    hidden = gate_w.shape[1]
    bits = [1 << b for b in range(narrow.bit_length() - 1)]

    def swap(value, mask):
        return lax.ppermute(value, "tp", [(i, i ^ mask) for i in range(narrow)])

    def exchange(value):
        return lax.all_to_all(value, "sp", split_axis=0, concat_axis=0, tiled=True)

    part_rows, part_cot = pl.pallas_call(
        functools.partial(dispatch_kernel, experts=experts, share=share),
        out_shape=[jax.ShapeDtypeStruct((picks, width), BF16)] * 2,
        in_specs=[smem(), vmem(), vmem(), vmem(), vmem()],
        out_specs=[vmem(), vmem()],
        name="dispatch",
    )(me_arr, routes, route_weights, layer_input, out_cot)
    got_rows = exchange(part_rows.reshape(experts, share, width)).reshape(picks, width)
    got_cot = exchange(part_cot.reshape(experts, share, width)).reshape(picks, width)

    def spread_over_tp(value):
        found = [value]
        for bit in reversed(bits):
            found = found + [swap(v, bit) for v in found]
        return found

    masks = [0]
    for bit in reversed(bits):
        masks = masks + [m | bit for m in masks]
    rows = spread_over_tp(got_rows)
    cots = spread_over_tp(got_cot)

    act, fac_gate, fac_up = pl.pallas_call(
        functools.partial(hidden_kernel, parts=narrow),
        out_shape=[
            jax.ShapeDtypeStruct((narrow, picks, hidden), BF16),
            jax.ShapeDtypeStruct((narrow, picks, hidden), F32),
            jax.ShapeDtypeStruct((narrow, picks, hidden), F32),
        ],
        in_specs=[vmem()] * (narrow + 2),
        out_specs=[vmem()] * 3,
        cost_estimate=cost(4 * narrow * picks * width * hidden, 6e6),
        name="hidden",
    )(*rows, gate_w, up_w)

    position = {m: p for p, m in enumerate(masks)}
    orders = [(m, [position[masks[p] ^ m] for p in range(narrow)]) for m in range(narrow)]
    back = pl.pallas_call(
        functools.partial(back_kernel, parts=narrow, orders=orders),
        out_shape=[jax.ShapeDtypeStruct((narrow, picks, hidden), BF16)] * 2
        + [jax.ShapeDtypeStruct((narrow, picks, cols), BF16 if m & 1 else F32) for m in range(narrow)],
        in_specs=[smem()] + [vmem()] * (narrow + 5),
        out_specs=[vmem()] * (narrow + 2),
        cost_estimate=cost(6 * narrow * picks * width * hidden, 12e6),
        name="back",
    )(me_arr, *cots, down_w, fac_gate, fac_up, gate_w, up_w)
    d_gate, d_up, partial = back[0], back[1], list(back[2:])
    for bit in bits:
        count = narrow // bit
        for m in reversed(range(0, narrow, 2 * bit)):
            received = swap(partial[m + bit].astype(BF16), bit)
            partial[m] = partial[m].astype(F32) + received.astype(F32)
    returning = (
        partial[0]
        .astype(BF16)
        .reshape(narrow, experts, share, cols)
        .transpose(1, 0, 2, 3)
        .reshape(experts, capacity, cols)
    )
    returned = exchange(returning).reshape(experts * capacity, cols)
    cot_cols = pl.pallas_call(
        functools.partial(combine_kernel, experts=experts, share=share, masks=masks),
        out_shape=jax.ShapeDtypeStruct((tok_rows, cols), BF16),
        grid_spec=pltpu.PrefetchScalarGridSpec(
            num_scalar_prefetch=1,
            grid=(1,),
            in_specs=[
                pl.BlockSpec(routes.shape, lambda i, s: (0, 0)),
                pl.BlockSpec((tok_rows, cols), lambda i, s: (0, s[0])),
                pl.BlockSpec(returned.shape, lambda i, s: (0, 0)),
            ],
            out_specs=pl.BlockSpec((tok_rows, cols), lambda i, s: (0, 0)),
        ),
        name="combine",
    )(me_arr, routes, out_cot, returned)
    mixer_cot = lax.all_gather(cot_cols, "tp", axis=1, tiled=True)

    all_rows = jnp.concatenate(rows, 0)
    all_cots = jnp.concatenate(cots, 0)
    grad_gate = dot(all_rows, d_gate.reshape(-1, hidden), TN).astype(BF16)[None]
    grad_up = dot(all_rows, d_up.reshape(-1, hidden), TN).astype(BF16)[None]
    grad_down = dot(act.reshape(-1, hidden), all_cots, TN).astype(BF16)[None]

    heads = queries.shape[1] // DK
    head_ids = (me * heads + jnp.arange(heads, dtype=jnp.int32)).astype(F32)
    rates = decay_rates(head_ids, heads * narrow, tok_rows * experts)
    positions = (here * tok_rows + jnp.arange(tok_rows, dtype=jnp.int32)).astype(F32)
    norm = jnp.repeat(position_norm(positions, rates), DK, axis=1)
    head_cot = (dot(mixer_cot, out_proj) * norm).astype(BF16)
    split = (tok_rows, heads, DK)
    query, key, value, cot = (x.reshape(split) for x in (queries, keys, values, head_cot))
    scale = DK ** (-0.5)
    offsets = jnp.arange(SPAN, dtype=F32)
    distance = offsets[:, None] - offsets[None, :]
    decay = jnp.where(
        distance[None] >= 0, jnp.exp(-rates[:, None, None] * jnp.maximum(distance, 0.0)[None]), 0.0
    )
    tail = jnp.exp(-rates[None, :] * (SPAN - 1.0 - offsets)[:, None])[:, :, None]
    lead = jnp.exp(-rates[None, :] * (offsets + 1.0)[:, None])[:, :, None]

    def ein(spec, a, b):
        return jnp.einsum(spec, a, b, preferred_element_type=F32)

    local = ein("ihd,ihe->dhe", (query.astype(F32) * lead).astype(BF16), cot)
    sent = jnp.broadcast_to(local.astype(BF16).reshape(1, DK, heads * DK), (experts, DK, heads * DK))
    states = exchange(sent)
    ahead = jnp.arange(experts, dtype=jnp.int32) - here
    steps = jnp.exp(-rates[None, :] * (tok_rows * jnp.maximum(ahead - 1, 0)).astype(F32)[:, None])
    steps = jnp.repeat(jnp.where(ahead[:, None] > 0, steps, 0.0), DK, axis=1)
    reverse = jnp.sum(states.astype(F32) * steps[:, None, :], axis=0).astype(BF16).reshape(DK, heads, DK)

    mixed = mixer_out
    mixed, _ = lax.optimization_barrier((mixer_out, got_cot))
    mixed_all = exchange(jnp.broadcast_to(mixed[None], (experts, *mixed.shape))).reshape(-1, mixed.shape[1])
    cot_slice = lax.all_to_all(mixer_cot, "sp", split_axis=1, concat_axis=0, tiled=True)
    grad_proj = dot(cot_slice, mixed_all, TN)

    fwd = (ein("ihd,jhd->hij", query, key) * scale * decay).astype(BF16)
    bwd = (ein("ihd,jhd->hij", cot, value) * decay).astype(BF16)
    grad_q = scale * ein("hij,jhd->ihd", bwd, key) + lead * ein(
        "hde,ihe->ihd", entry_states[0].astype(BF16), cot
    )
    grad_k = scale * (ein("hij,ihd->jhd", bwd, query) + tail * ein("dhe,jhe->jhd", reverse, value))
    grad_v = ein("hij,ihe->jhe", fwd, cot) + scale * tail * ein("dhe,jhd->jhe", reverse, key)
    flat = (tok_rows, heads * DK)
    return (
        grad_gate,
        grad_up,
        grad_down,
        grad_proj,
        grad_q.reshape(flat).astype(BF16),
        grad_k.reshape(flat).astype(BF16),
        grad_v.reshape(flat).astype(BF16),
    )


def solution(mesh):
    return jax.shard_map(
        per_device,
        mesh=mesh,
        in_specs=(
            P("sp", None),
            P("sp", None),
            P("sp", None),
            P("sp", None),
            P("sp", None, "tp"),
            P("sp", None, "tp"),
            P("sp", "tp", None),
            P(None, "tp"),
            P("sp", "tp"),
            P("sp", "tp"),
            P("sp", "tp"),
            P("sp", "tp"),
            P("sp", "tp", None, None),
        ),
        out_specs=(
            P("sp", None, "tp"),
            P("sp", None, "tp"),
            P("sp", "tp", None),
            P("sp", "tp"),
            P("sp", "tp"),
            P("sp", "tp"),
            P("sp", "tp"),
        ),
        check_vma=False,
    )
```

time: 316 us -> 196 us (0.62)
  waiting for transfers between devices: 170 us -> 83 us
  blocking collectives: 65.2 us -> 29.2 us
  starting transfers between devices: 5.69 us -> 26.3 us
  Pallas kernels: 0 us -> 17.7 us
  between operations: 14.2 us -> 1 us
  other arithmetic: 15.2 us -> 4.94 us
  matrix products: 25.4 us -> 17.1 us
  local copies, waits for them, and re-layouts: 19.2 us -> 15.9 us
    reduce_scatter x2 -> x0, waiting for transfers between devices: 124 us -> none  [the longest x1 79.2 us: per_device(): lax.psum_scatter(lax.dot_general(mixer_cot, mixer_out, (((0,), (0,)), (()...]
    all_to_all x1 -> x5, waiting for transfers between devices: 13.9 us -> 58.3 us  [the longest x4 49.6 us: exchange(): return lax.all_to_all(value, 'sp', split_axis=0, concat_axis=0, tiled=True)]
    all_gather x3 -> x0, waiting for transfers between devices: 32.6 us -> none  [the longest x1 16.7 us: per_device(): lax.all_gather(got_cot, 'tp', axis=1, tiled=True)]
    ppermute x0 -> x9, waiting for transfers between devices: none -> 24.7 us  [swap(): return lax.ppermute(value, 'tp', [(i, i ^ mask) for i in range(narrow)])]
    all_gather x1 -> x0, blocking collectives: 19.2 us -> none  [prefix(): everything = jax.tree.map(lambda part: lax.all_gather(part, axis), array)]
    pallas_call x0 -> x4, Pallas kernels: none -> 17.7 us  [the longest x1 7.82 us: per_device(): pl.pallas_call(functools.partial(back_kernel, parts=narrow, orders=orders...]
    all_to_all x2 -> x1, blocking collectives: 39.3 us -> 21.8 us  [exchange(): return lax.all_to_all(value, 'sp', split_axis=0, concat_axis=0, tiled=True)]
    all_to_all x1 -> x5, starting transfers between devices: 5.49 us -> 20.6 us  [the longest x4 17 us: exchange(): return lax.all_to_all(value, 'sp', split_axis=0, concat_axis=0, tiled=True)]
  transfers between devices with their start and end apart: 6 -> 14, of which waited for: 5 -> 8; matrix products, arithmetic and copies ran while one was open for 11% -> 13% of each run, Pallas kernels for 0% -> 2%
where the time goes in v1:
time: 196 us; the launch traced here: 195 us
  waiting for transfers between devices  83 us (42%)
  blocking collectives  29.2 us (15%)
  starting transfers between devices  26.3 us (13%)
  Pallas kernels  17.7 us (9%)
  matrix products  17.1 us (9%)
  local copies, waits for them, and re-layouts  15.9 us (8%)
  other arithmetic  4.94 us (3%)
    all_to_all x4, waiting for transfers between devices, exchange(): return lax.all_to_all(value, 'sp', split_axis=0, concat_axis=0, tiled=True)  49.6 us
    ppermute x9, waiting for transfers between devices, swap(): return lax.ppermute(value, 'tp', [(i, i ^ mask) for i in range(narrow)])  24.7 us
    all_to_all x1, blocking collectives, exchange(): return lax.all_to_all(value, 'sp', split_axis=0, concat_axis=0, tiled=True)  21.8 us
    all_to_all x4, starting transfers between devices, exchange(): return lax.all_to_all(value, 'sp', split_axis=0, concat_axis=0, tiled=True)  17 us
    dot_general x5, matrix products, dot(): lax.dot_general(a, b, dims, precision=precision, preferred_element_type=F32)  11.8 us
    unnamed x52, local copies, waits for them, and re-layouts  10.6 us
    all_to_all x1, waiting for transfers between devices, per_device(): lax.all_to_all(mixer_cot, 'sp', split_axis=1, concat_axis=0, tiled=True)  8.76 us
    pallas_call x1, Pallas kernels, per_device(): pl.pallas_call(functools.partial(back_kernel, parts=narrow, orders=orders...  7.82 us
  transfers between devices with their start and end apart: 14, of which 8 were waited for; matrix products, arithmetic and copies ran while one was open for 13% of the time, Pallas kernels for 2%

profile of v1, /device:TPU:0, one launch (start us, length us, event | category | flops | bytes accessed | tf_op | source)
XLA Modules:
  0.0 195.1 jit_solution(12121238336042773025)
XLA Ops:
  3.6 3.0 %dispatch.1 = (bf16[128,2048]{1,0:T(8,128)(2,1)}, bf16[128,2048]{1,0:T(8,128)(2,1)}) custom-call(s32[1]{0:T(128)} %bitcast.me_ref, s32[128,2]{1,0:T(8,128)} %copy.54.routes_ref, f32[128,2]{1,0:T(8,128)} %copy.55.weights_ref, bf16[128,2048]{1,0:T(8,128)(2,1)} %rows_ref.1, bf16[128,2048]{1,0:T(8,128)(2,1)} %cot_ref.3), custom_call_target="tpu_custom_call" | custom-call | tf_op jit(solution)/shard_map/dispatch/pallas_call | solution.py:175
  6.6 21.8 %all_to_all.41 = bf16[8,16,2048]{2,1,0:T(8,128)(2,1)S(1)} all-to-all(bf16[8,16,2048]{2,1,0:T(8,128)(2,1)} %bitcast.127), channel_id=1, replica_groups=mesh['sp'=8,'tp'=4] {'sp'}, dimensions={0} | all-to-all | bytes 1048576 | tf_op jit(solution)/shard_map/all_to_all | solution.py:173
  28.4 3.6 %all-to-all-start.1 = ((bf16[8,16,2048]{2,1,0:T(8,128)(2,1)}), bf16[8,16,2048]{2,1,0:T(8,128)(2,1)S(1)}, u32[]{:S(2)}, u32[]{:S(2)}) async-start(bf16[8,16,2048]{2,1,0:T(8,128)(2,1)} %bitcast.126), calls=%async_computation.1 | async-start | bytes 1048576 | tf_op jit(solution)/shard_map/all_to_all | solution.py:173
  33.5 12.6 %all-to-all-done.1 = bf16[8,16,2048]{2,1,0:T(8,128)(2,1)S(1)} async-done(((bf16[8,16,2048]{2,1,0:T(8,128)(2,1)}), bf16[8,16,2048]{2,1,0:T(8,128)(2,1)S(1)}, u32[]{:S(2)}, u32[]{:S(2)}) %all-to-all-start.1) | async-done | bytes 524320 | tf_op jit(solution)/shard_map/all_to_all | solution.py:173
  48.2 10.3 %collective-permute-done.3.refs_1_ = bf16[128,2048]{1,0:T(8,128)(2,1)} collective-permute-done((bf16[128,2048]{1,0:T(8,128)(2,1)S(1)}, bf16[128,2048]{1,0:T(8,128)(2,1)}, u32[]{:S(2)}, u32[]{:S(2)}) %collective-permute-start.3) | collective-permute-done | bytes 524320 | tf_op jit(solution)/shard_map/ppermute | solution.py:170
  60.2 4.5 %hidden.1 = (bf16[4,128,256]{2,1,0:T(8,128)(2,1)}, f32[4,128,256]{2,1,0:T(8,128)}, f32[4,128,256]{2,1,0:T(8,128)}) custom-call(bf16[128,2048]{1,0:T(8,128)(2,1)} %bitcast.108, bf16[128,2048]{1,0:T(8,128)(2,1)} %collective-permute-done.refs_1_, bf16[128,2048]{1,0:T(8,128)(2,1)} %copy-done.8, bf16[128,2048]{1,0:T(8,128)(2,1)} %copy-done.10, ...), custom_call_target="tpu_custom_call" | custom-call | flops 1073741824 | bytes 6000000 | tf_op jit(solution)/shard_map/hidden/pallas_call | solution.py:197
  64.7 7.8 %back.1 = (bf16[4,128,256]{2,1,0:T(8,128)(2,1)}, bf16[4,128,256]{2,1,0:T(8,128)(2,1)}, f32[4,128,512]{2,1,0:T(8,128)}, bf16[4,128,512]{2,1,0:T(8,128)(2,1)}, f32...) custom-call(s32[1]{0:T(128)} %bitcast.me_ref, bf16[128,2048]{1,0:T(8,128)(2,1)} %bitcast.102, ...), custom_call_target="tpu_custom_call" | custom-call | flops 1610612736 | bytes 12000000 | tf_op jit(solution)/shard_map/back/pallas_call | solution.py:212
  73.1 1.7 collective-permute-done.7
  77.8 12.7 %collective-permute-done.8 = bf16[4,128,512]{2,1,0:T(8,128)(2,1)S(1)} collective-permute-done((bf16[4,128,512]{2,1,0:T(8,128)(2,1)S(1)}, bf16[4,128,512]{2,1,0:T(8,128)(2,1)S(1)}, u32[]{:S(2)}, u32[]{:S(2)}) %collective-permute-start.8) | collective-permute-done | bytes 524320 | tf_op jit(solution)/shard_map/ppermute | solution.py:170
  91.5 5.0 %all-to-all-start.2 = ((bf16[8,64,512]{2,1,0:T(8,128)(2,1)}), bf16[8,64,512]{2,1,0:T(8,128)(2,1)S(1)}, u32[]{:S(2)}, u32[]{:S(2)}) async-start(bf16[8,64,512]{2,1,0:T(8,128)(2,1)} %bitcast.16), calls=%async_computation.2 | async-start | bytes 1048576 | tf_op jit(solution)/shard_map/all_to_all | solution.py:173
  97.7 13.1 %all-to-all-done.2 = bf16[8,64,512]{2,1,0:T(8,128)(2,1)S(1)} async-done(((bf16[8,64,512]{2,1,0:T(8,128)(2,1)}), bf16[8,64,512]{2,1,0:T(8,128)(2,1)S(1)}, u32[]{:S(2)}, u32[]{:S(2)}) %all-to-all-start.2) | async-done | bytes 524320 | tf_op jit(solution)/shard_map/all_to_all | solution.py:173
  111.5 2.4 %combine.1 = bf16[128,512]{1,0:T(8,128)(2,1)} custom-call(s32[1]{0:T(128)} %bitcast.me_ref, s32[128,2]{1,0:T(8,128)} %copy.54.routes_ref, bf16[128,2048]{1,0:T(8,128)(2,1)} %cot_ref.3, bf16[512,512]{1,0:T(8,128)(2,1)} %bitcast.105), custom_call_target="tpu_custom_call" | custom-call | tf_op jit(solution)/shard_map/combine/pallas_call | solution.py:235
  113.9 7.4 %all_gather.3 = bf16[128,2048]{1,0:T(8,128)(2,1)S(1)} all-gather(bf16[128,512]{1,0:T(8,128)(2,1)} %combine.1), channel_id=1, replica_groups=mesh['sp'=8,'tp'=4] {'tp'}, dimensions={1}, use_global_device_ids=true | all-gather | bytes 655360 | tf_op jit(solution)/shard_map/all_gather | solution.py:250
  123.0 4.2 %all-to-all-start.5 = ((bf16[8,64,512]{2,1,0:T(8,128)(2,1)}), bf16[8,64,512]{2,1,0:T(8,128)(2,1)}, u32[]{:S(2)}, u32[]{:S(2)}) async-start(bf16[8,64,512]{2,1,0:T(8,128)(2,1)} %broadcast_in_dim.77), calls=%async_computation.5 | async-start | bytes 1048576 | tf_op jit(solution)/shard_map/all_to_all | solution.py:173
  131.5 11.0 %all-to-all-done.5 = bf16[8,64,512]{2,1,0:T(8,128)(2,1)} async-done(((bf16[8,64,512]{2,1,0:T(8,128)(2,1)}), bf16[8,64,512]{2,1,0:T(8,128)(2,1)}, u32[]{:S(2)}, u32[]{:S(2)}) %all-to-all-start.5) | async-done | bytes 524320 | tf_op jit(solution)/shard_map/all_to_all | solution.py:173
  142.5 2.0 %broadcast_in_dim.43 = bf16[8,128,512]{2,1,0:T(8,128)(2,1)} broadcast(bf16[128,512]{1,0:T(8,128)(2,1)} %param.24), dimensions={1,2} | broadcast | bytes 1179648 | tf_op jit(solution)/shard_map/broadcast_in_dim | solution.py:288
  144.4 4.2 %all-to-all-start.4 = ((bf16[8,128,512]{2,1,0:T(8,128)(2,1)}), bf16[8,128,512]{2,1,0:T(8,128)(2,1)}, u32[]{:S(2)}, u32[]{:S(2)}) async-start(bf16[8,128,512]{2,1,0:T(8,128)(2,1)} %broadcast_in_dim.43), calls=%async_computation.4 | async-start | bytes 2097152 | tf_op jit(solution)/shard_map/all_to_all | solution.py:173
  148.8 3.3 %fusion.2 = bf16[1,256,2048]{2,1,0:T(8,128)(2,1)} fusion(bf16[512,256]{1,0:T(8,128)(2,1)} %bitcast.133, bf16[128,2048]{1,0:T(8,128)(2,1)} %collective-permute-done.5.refs_3_, bf16[128,2048]{1,0:T(8,128)(2,1)} %collective-permute-done.4.refs_2_, bf16[128,2048]{1,0:T(8,128)(2,1)} %collective-permute-done.3.refs_1_, bf16[128,2048]{1,0:T(8,128)(2,1)S(1)} %bitcast.103), kind=kOutput, calls=%fused_computation.5 | convolution fusion | flops 545783808 | bytes 3407872 | tf_op jit(solution)/shard_map/dot_general | solution.py:20
  152.0 2.8 %fusion.1 = bf16[1,2048,256]{2,1,0:T(8,128)(2,1)} fusion(bf16[512,256]{1,0:T(8,128)(2,1)S(1)} %bitcast.135, bf16[128,2048]{1,0:T(8,128)(2,1)S(1)} %copy-done.11, bf16[128,2048]{1,0:T(8,128)(2,1)S(1)} %copy-done.9, bf16[128,2048]{1,0:T(8,128)(2,1)} %collective-permute-done.refs_1_, bf16[128,2048]{1,0:T(8,128)(2,1)S(1)} %bitcast.109), kind=kOutput, calls=%fused_computation.4 | convolution fusion | flops 545783808 | bytes 3407872 | tf_op jit(solution)/shard_map/dot_general | solution.py:20
  154.9 2.8 %fusion = bf16[1,2048,256]{2,1,0:T(8,128)(2,1)} fusion(bf16[512,256]{1,0:T(8,128)(2,1)S(1)} %bitcast.134, bf16[128,2048]{1,0:T(8,128)(2,1)S(1)} %copy-done.11, bf16[128,2048]{1,0:T(8,128)(2,1)S(1)} %copy-done.9, bf16[128,2048]{1,0:T(8,128)(2,1)} %collective-permute-done.refs_1_, bf16[128,2048]{1,0:T(8,128)(2,1)S(1)} %bitcast.110), kind=kOutput, calls=%fused_computation.3 | convolution fusion | flops 545783808 | bytes 3407872 | tf_op jit(solution)/shard_map/dot_general | solution.py:20
  161.6 12.8 %all-to-all-done.4 = bf16[8,128,512]{2,1,0:T(8,128)(2,1)} async-done(((bf16[8,128,512]{2,1,0:T(8,128)(2,1)}), bf16[8,128,512]{2,1,0:T(8,128)(2,1)}, u32[]{:S(2)}, u32[]{:S(2)}) %all-to-all-start.4) | async-done | bytes 1048608 | tf_op jit(solution)/shard_map/all_to_all | solution.py:173
  174.4 3.6 %all-to-all-start.3 = ((bf16[128,8,256]{0,2,1:T(8,128)(2,1)}), bf16[128,8,256]{0,2,1:T(8,128)(2,1)S(1)}, u32[]{:S(2)}, u32[]{:S(2)}) async-start(bf16[128,8,256]{0,2,1:T(8,128)(2,1)} %bitcast.18), calls=%async_computation.3 | async-start | bytes 1048576 | tf_op jit(solution)/shard_map/all_to_all | solution.py:289
  183.9 8.8 %all-to-all-done.3 = bf16[128,8,256]{0,2,1:T(8,128)(2,1)S(1)} async-done(((bf16[128,8,256]{0,2,1:T(8,128)(2,1)}), bf16[128,8,256]{0,2,1:T(8,128)(2,1)S(1)}, u32[]{:S(2)}, u32[]{:S(2)}) %all-to-all-start.3) | async-done | bytes 524320 | tf_op jit(solution)/shard_map/all_to_all | solution.py:289
  192.6 2.5 %convolution_bitcast_fusion = f32[256,512]{1,0:T(8,128)} fusion(bf16[8,128,512]{2,1,0:T(8,128)(2,1)} %all-to-all-done.4, bf16[128,8,256]{0,2,1:T(8,128)(2,1)S(1)} %all-to-all-done.3), kind=kOutput, calls=%fused_computation.16 | convolution fusion | flops 268435456 | bytes 2097152 | tf_op jit(solution)/shard_map/dot_general | solution.py:20
  (100 shorter events, 30.3 us)
Async XLA Ops:
  0.6 120.7 %copy-start = (bf16[2048,512]{1,0:T(8,128)(2,1)S(1)}, bf16[2048,512]{1,0:T(8,128)(2,1)}, u32[]{:S(2)}) copy-start(bf16[2048,512]{1,0:T(8,128)(2,1)} %param.20) | copy-start | bytes 6291460
  28.4 31.7 %copy-start.4 = (bf16[8,16,2048]{2,1,0:T(8,128)(2,1)}, bf16[8,16,2048]{2,1,0:T(8,128)(2,1)S(1)}, u32[]{:S(2)}) copy-start(bf16[8,16,2048]{2,1,0:T(8,128)(2,1)S(1)} %all_to_all.41) | copy-start | bytes 1572868
  28.4 17.8 %all-to-all-start.1 = ((bf16[8,16,2048]{2,1,0:T(8,128)(2,1)}), bf16[8,16,2048]{2,1,0:T(8,128)(2,1)S(1)}, u32[]{:S(2)}, u32[]{:S(2)}) async-start(bf16[8,16,2048]{2,1,0:T(8,128)(2,1)} %bitcast.126), calls=%async_computation.1 | async-start | bytes 1048576 | tf_op jit(solution)/shard_map/all_to_all | solution.py:173
  32.0 15.7 %collective-permute-start = (bf16[128,2048]{1,0:T(8,128)(2,1)S(1)}, bf16[128,2048]{1,0:T(8,128)(2,1)}, u32[]{:S(2)}, u32[]{:S(2)}) collective-permute-start(bf16[128,2048]{1,0:T(8,128)(2,1)S(1)} %bitcast.106), channel_id=1, source_target_pairs={{0,2},{1,3},{2,0},{3,1},{4,6},{5,7},{6,4},{7,5},{8,10},{9,11},{10,... | collective-permute-start | bytes 1572872 | tf_op jit(solution)/shard_map/ppermute | solution.py:170
  46.2 18.5 %copy-start.1 = (bf16[8,16,2048]{2,1,0:T(8,128)(2,1)}, bf16[8,16,2048]{2,1,0:T(8,128)(2,1)S(1)}, u32[]{:S(2)}) copy-start(bf16[8,16,2048]{2,1,0:T(8,128)(2,1)S(1)} %all-to-all-done.1) | copy-start | bytes 1572868
  46.2 12.3 %collective-permute-start.3 = (bf16[128,2048]{1,0:T(8,128)(2,1)S(1)}, bf16[128,2048]{1,0:T(8,128)(2,1)}, u32[]{:S(2)}, u32[]{:S(2)}) collective-permute-start(bf16[128,2048]{1,0:T(8,128)(2,1)S(1)} %bitcast.100), channel_id=1, source_target_pairs={{0,2},{1,3},{2,0},{3,1},{4,6},{5,7},{6,4},{7,5},{8,10},{9,11},{10,... | collective-permute-start | bytes 1572872 | tf_op jit(solution)/shard_map/ppermute | solution.py:170
  47.7 10.8 %collective-permute-start.1 = (bf16[128,2048]{1,0:T(8,128)(2,1)S(1)}, bf16[128,2048]{1,0:T(8,128)(2,1)S(1)}, u32[]{:S(2)}, u32[]{:S(2)}) collective-permute-start(bf16[128,2048]{1,0:T(8,128)(2,1)S(1)} %bitcast.107), channel_id=1, source_target_pairs={{0,1},{1,0},{2,3},{3,2},{4,5},{5,4},{6,7},{7,6},{8,9},{9,8},{10,11... | collective-permute-start | bytes 1572872 | tf_op jit(solution)/shard_map/ppermute | solution.py:170
  47.7 11.6 %collective-permute-start.2 = (bf16[128,2048]{1,0:T(8,128)(2,1)}, bf16[128,2048]{1,0:T(8,128)(2,1)S(1)}, u32[]{:S(2)}, u32[]{:S(2)}) collective-permute-start(bf16[128,2048]{1,0:T(8,128)(2,1)} %collective-permute-done.refs_1_), channel_id=1, source_target_pairs={{0,1},{1,0},{2,3},{3,2},{4,5},{5,4},{6,7},{7,6},{8,9},{9,8},{10,11... | collective-permute-start | bytes 1572872 | tf_op jit(solution)/shard_map/ppermute | solution.py:170
  48.2 16.5 %collective-permute-start.4 = (bf16[128,2048]{1,0:T(8,128)(2,1)S(1)}, bf16[128,2048]{1,0:T(8,128)(2,1)}, u32[]{:S(2)}, u32[]{:S(2)}) collective-permute-start(bf16[128,2048]{1,0:T(8,128)(2,1)S(1)} %bitcast.101), channel_id=1, source_target_pairs={{0,1},{1,0},{2,3},{3,2},{4,5},{5,4},{6,7},{7,6},{8,9},{9,8},{10,11... | collective-permute-start | bytes 1572872 | tf_op jit(solution)/shard_map/ppermute | solution.py:170
  58.5 6.2 %collective-permute-start.5 = (bf16[128,2048]{1,0:T(8,128)(2,1)}, bf16[128,2048]{1,0:T(8,128)(2,1)}, u32[]{:S(2)}, u32[]{:S(2)}) collective-permute-start(bf16[128,2048]{1,0:T(8,128)(2,1)} %collective-permute-done.3.refs_1_), channel_id=1, source_target_pairs={{0,1},{1,0},{2,3},{3,2},{4,5},{5,4},{6,7},{7,6},{8,9},{9,8},{10,11... | collective-permute-start | bytes 1572872 | tf_op jit(solution)/shard_map/ppermute | solution.py:170
  72.5 17.9 %copy-start.6 = (f32[4,128,512]{2,1,0:T(8,128)S(1)}, f32[4,128,512]{2,1,0:T(8,128)}, u32[]{:S(2)}) copy-start(f32[4,128,512]{2,1,0:T(8,128)} %get-tuple-element.26) | copy-start | bytes 3145732
  72.5 2.2 %collective-permute-start.7 = (bf16[4,128,512]{2,1,0:T(8,128)(2,1)}, bf16[4,128,512]{2,1,0:T(8,128)(2,1)S(1)}, u32[]{:S(2)}, u32[]{:S(2)}) collective-permute-start(bf16[4,128,512]{2,1,0:T(8,128)(2,1)} %get-tuple-element.29), channel_id=1, source_target_pairs={{0,1},{1,0},{2,3},{3,2},{4,5},{5,4},{6,7},{7,6},{8,9},{9,8},{10,11... | collective-permute-start | bytes 1572872 | tf_op jit(solution)/shard_map/ppermute | solution.py:170
  73.0 4.7 %collective-permute-start.6 = (bf16[4,128,512]{2,1,0:T(8,128)(2,1)}, bf16[4,128,512]{2,1,0:T(8,128)(2,1)S(1)}, u32[]{:S(2)}, u32[]{:S(2)}) collective-permute-start(bf16[4,128,512]{2,1,0:T(8,128)(2,1)} %get-tuple-element.27), channel_id=1, source_target_pairs={{0,1},{1,0},{2,3},{3,2},{4,5},{5,4},{6,7},{7,6},{8,9},{9,8},{10,11... | collective-permute-start | bytes 1572872 | tf_op jit(solution)/shard_map/ppermute | solution.py:170
  76.2 14.3 %collective-permute-start.8 = (bf16[4,128,512]{2,1,0:T(8,128)(2,1)S(1)}, bf16[4,128,512]{2,1,0:T(8,128)(2,1)S(1)}, u32[]{:S(2)}, u32[]{:S(2)}) collective-permute-start(bf16[4,128,512]{2,1,0:T(8,128)(2,1)S(1)} %add_convert_fusion.1), channel_id=1, source_target_pairs={{0,2},{1,3},{2,0},{3,1},{4,6},{5,7},{6,4},{7,5},{8,10},{9,11},{10,... | collective-permute-start | bytes 1572872 | tf_op jit(solution)/shard_map/ppermute | solution.py:170
  90.7 6.2 %copy-start.13 = (bf16[128,512]{1,0:T(8,128)(2,1)S(1)}, bf16[128,512]{1,0:T(8,128)(2,1)}, u32[]{:S(2)}) copy-start(bf16[128,512]{1,0:T(8,128)(2,1)} %param.21) | copy-start | bytes 393220
  91.5 19.2 %all-to-all-start.2 = ((bf16[8,64,512]{2,1,0:T(8,128)(2,1)}), bf16[8,64,512]{2,1,0:T(8,128)(2,1)S(1)}, u32[]{:S(2)}, u32[]{:S(2)}) async-start(bf16[8,64,512]{2,1,0:T(8,128)(2,1)} %bitcast.16), calls=%async_computation.2 | async-start | bytes 1048576 | tf_op jit(solution)/shard_map/all_to_all | solution.py:173
  96.6 30.7 %copy-start.18 = (f32[8]{0:T(128)}, f32[8]{0:T(128)S(1)}, u32[]{:S(2)}) copy-start(f32[8]{0:T(128)S(1)} %get-tuple-element.56) | copy-start | bytes 100
  97.7 25.4 %copy-start.15 = (f32[128,8]{0,1:T(8,128)}, f32[128,8]{0,1:T(8,128)S(1)}, u32[]{:S(2)}) copy-start(f32[128,8]{0,1:T(8,128)S(1)} %get-tuple-element.54) | copy-start | bytes 12292
  123.0 19.4 %all-to-all-start.5 = ((bf16[8,64,512]{2,1,0:T(8,128)(2,1)}), bf16[8,64,512]{2,1,0:T(8,128)(2,1)}, u32[]{:S(2)}, u32[]{:S(2)}) async-start(bf16[8,64,512]{2,1,0:T(8,128)(2,1)} %broadcast_in_dim.77), calls=%async_computation.5 | async-start | bytes 1048576 | tf_op jit(solution)/shard_map/all_to_all | solution.py:173
  127.2 21.5 %copy-start.2 = (bf16[8,16,2048]{2,1,0:T(8,128)(2,1)S(1)}, bf16[8,16,2048]{2,1,0:T(8,128)(2,1)}, u32[]{:S(2)}) copy-start(bf16[8,16,2048]{2,1,0:T(8,128)(2,1)} %copy-done.1) | copy-start | bytes 1572868
  144.4 30.0 %all-to-all-start.4 = ((bf16[8,128,512]{2,1,0:T(8,128)(2,1)}), bf16[8,128,512]{2,1,0:T(8,128)(2,1)}, u32[]{:S(2)}, u32[]{:S(2)}) async-start(bf16[8,128,512]{2,1,0:T(8,128)(2,1)} %broadcast_in_dim.43), calls=%async_computation.4 | async-start | bytes 2097152 | tf_op jit(solution)/shard_map/all_to_all | solution.py:173
  154.9 3.9 %copy-start.17 = (pred[128,128]{1,0:T(8,128)(4,1)S(1)}, pred[128,128]{1,0:T(8,128)(4,1)}, u32[]{:S(2)}) copy-start(pred[128,128]{1,0:T(8,128)(4,1)} %fusion.35) | copy-start | bytes 49156
  154.9 4.2 %copy-start.16 = (f32[128,8]{0,1:T(8,128)S(1)}, f32[128,8]{0,1:T(8,128)}, u32[]{:S(2)}) copy-start(f32[128,8]{0,1:T(8,128)} %copy-done.15) | copy-start | bytes 12292
  174.4 18.2 %all-to-all-start.3 = ((bf16[128,8,256]{0,2,1:T(8,128)(2,1)}), bf16[128,8,256]{0,2,1:T(8,128)(2,1)S(1)}, u32[]{:S(2)}, u32[]{:S(2)}) async-start(bf16[128,8,256]{0,2,1:T(8,128)(2,1)} %bitcast.18), calls=%async_computation.3 | async-start | bytes 1048576 | tf_op jit(solution)/shard_map/all_to_all | solution.py:289
  (12 other events, 31.3 us)

commit v2 on v1

v2 whole, which is shorter than its diff:
```python
import functools

import jax
import jax.numpy as jnp
from jax import lax
from jax.experimental import pallas as pl
from jax.experimental.pallas import tpu as pltpu
from jax.sharding import PartitionSpec as P


DK = 64
F32 = jnp.float32
BF16 = jnp.bfloat16
NN = (((1,), (0,)), ((), ()))
NT = (((1,), (1,)), ((), ()))
TN = (((0,), (0,)), ((), ()))


def dot(a, b, dims=NN, precision=None):
    return lax.dot_general(a, b, dims, precision=precision, preferred_element_type=F32)


def decay_rates(head_ids, head_count, token_count):
    half_count = head_count // 2
    fraction = jnp.minimum(head_ids, half_count) / half_count
    base_rate = jnp.exp(
        (1.0 - fraction) * jnp.log(1.0 / 32.0) + fraction * jnp.log(1.0 / token_count)
    )
    return base_rate * (1.0 + jnp.maximum(head_ids - half_count, 0.0) / half_count)


def position_norm(positions, head_rates):
    return jnp.sqrt(
        jnp.expm1(-2.0 * head_rates)[None, :]
        / jnp.expm1(-2.0 * head_rates[None, :] * (positions[:, None] + 1.0))
    )


def slot_table(routes, experts):
    top, tokens = routes.shape
    expert = lax.broadcasted_iota(jnp.int32, (experts, tokens), 0)
    named = jnp.zeros((experts, tokens), F32)
    for k in range(top):
        named = named + (routes[k : k + 1, :] == expert).astype(F32)
    row = lax.broadcasted_iota(jnp.int32, (tokens, tokens), 0)
    col = lax.broadcasted_iota(jnp.int32, (tokens, tokens), 1)
    earlier = dot(named.astype(BF16), (row < col).astype(BF16))
    return named * (earlier + 1.0), expert


def dispatch_kernel(
    me_ref, routes_ref, weights_ref, rows_hbm, cot_hbm, out_rows, out_cot, rows_ref, cot_ref, sems, *, experts, share
):
    copies = [
        pltpu.make_async_copy(rows_hbm, rows_ref, sems.at[0]),
        pltpu.make_async_copy(cot_hbm, cot_ref, sems.at[1]),
    ]
    for copy in copies:
        copy.start()
    routes = routes_ref[...]
    table, expert = slot_table(routes, experts)
    picks = experts * share
    top, tokens = routes.shape
    owner = lax.broadcasted_iota(jnp.int32, (picks, experts), 0) // share
    of_expert = (owner == lax.broadcasted_iota(jnp.int32, (picks, experts), 1)).astype(F32)
    spread = dot(of_expert.astype(BF16), table.astype(BF16))
    wanted = lax.broadcasted_iota(jnp.int32, (picks, tokens), 0) % share + me_ref[0] * share + 1
    chosen = spread == wanted.astype(F32)
    pick = chosen.astype(BF16)
    weight = jnp.zeros((experts, tokens), F32)
    for k in range(top):
        weight = weight + jnp.where(routes[k : k + 1, :] == expert, weights_ref[k : k + 1, :], 0.0)
    wide = dot(of_expert, weight, precision=lax.Precision.HIGHEST)
    slot_weight = jnp.sum(jnp.where(chosen, wide, 0.0), axis=1, keepdims=True)
    copies[0].wait()
    out_rows[...] = dot(pick, rows_ref[...]).astype(BF16)
    copies[1].wait()
    out_cot[...] = (slot_weight * dot(pick, cot_ref[...])).astype(BF16)


def places_kernel(me_ref, routes_ref, out_ref, *, experts, share, masks):
    table, _ = slot_table(routes_ref[...], experts)
    capacity = share * len(masks)
    picks = experts * capacity
    place = lax.broadcasted_iota(jnp.int32, (experts, picks), 1)
    of_expert = place // capacity == lax.broadcasted_iota(jnp.int32, (experts, picks), 0)
    spread = dot(table.astype(BF16), of_expert.astype(BF16), TN)
    at = lax.broadcasted_iota(jnp.int32, spread.shape, 1) % capacity
    part = at // share
    mask = jnp.zeros_like(part)
    for p, m in enumerate(masks):
        mask = jnp.where(part == p, m, mask)
    wanted = (mask ^ me_ref[0]) * share + at % share + 1
    out_ref[...] = (spread == wanted.astype(F32)).astype(BF16)


def hidden_kernel(*refs, parts):
    row_refs, (gate_hbm, up_hbm), (act_ref, fac_gate, fac_up) = refs[:parts], refs[parts : parts + 2], refs[parts + 2 : parts + 5]
    rows_buf, gate_ref, up_ref, sems = refs[parts + 5 :]
    weights = [
        pltpu.make_async_copy(gate_hbm, gate_ref, sems.at[parts]),
        pltpu.make_async_copy(up_hbm, up_ref, sems.at[parts + 1]),
    ]
    copies = [pltpu.make_async_copy(row_refs[p], rows_buf.at[p], sems.at[p]) for p in range(parts)]
    for copy in weights + copies:
        copy.start()
    for copy in weights:
        copy.wait()
    for p in range(parts):
        copies[p].wait()
        rows = rows_buf[p]
        gate_pre = dot(rows, gate_ref[...])
        up_pre = dot(rows, up_ref[...])
        sig = jax.nn.sigmoid(gate_pre)
        silu = gate_pre * sig
        act_ref[p] = (silu * up_pre).astype(BF16)
        fac_gate[p] = up_pre * sig * (1.0 + gate_pre * (1.0 - sig))
        fac_up[p] = silu


def put(out, order, value, parts):
    picks = value.shape[0] // parts
    for p in range(parts):
        piece = value[p * picks : (p + 1) * picks].astype(out.dtype)
        if out.ndim == 4:
            out[:, order[p]] = piece.reshape(out.shape[0], out.shape[2], out.shape[3])
        else:
            out[order[p]] = piece


def first_back_kernel(me_ref, *refs, parts, orders):
    cot_refs = refs[:parts]
    down_hbm, fg_hbm, fu_hbm, gate_hbm, up_hbm, dgate_ref, dup_ref, *outs = refs[parts : parts + 7 + len(orders)]
    cot_buf, down_ref, fac_gate, fac_up, gate_ref, up_ref, sems = refs[parts + 7 + len(orders) :]
    picks = cot_buf.shape[0] // parts
    cols = gate_ref.shape[1]
    copies = [pltpu.make_async_copy(down_hbm, down_ref, sems.at[parts])]
    copies += [pltpu.make_async_copy(cot_refs[p], cot_buf.at[pl.ds(p * picks, picks)], sems.at[p]) for p in range(parts)]
    copies += [
        pltpu.make_async_copy(fg_hbm, fac_gate, sems.at[parts + 1]),
        pltpu.make_async_copy(fu_hbm, fac_up, sems.at[parts + 2]),
    ]
    late = []
    for k, (mask, _) in enumerate(orders):
        first = pl.multiple_of((me_ref[0] ^ mask) * cols, cols)
        late.append(pltpu.make_async_copy(gate_hbm.at[pl.ds(first, cols)], gate_ref.at[k], sems.at[parts + 3 + 2 * k]))
        late.append(pltpu.make_async_copy(up_hbm.at[pl.ds(first, cols)], up_ref.at[k], sems.at[parts + 4 + 2 * k]))
    for copy in copies + late:
        copy.start()
    for copy in copies:
        copy.wait()
    d_act = dot(cot_buf[...], down_ref[...], NT)
    grads = []
    for fac, ref in ((fac_gate, dgate_ref), (fac_up, dup_ref)):
        grad = (d_act * fac[...].reshape(d_act.shape)).astype(BF16)
        ref[...] = grad.reshape(ref.shape)
        grads.append(grad)
    for k, (_, order) in enumerate(orders):
        late[2 * k].wait()
        late[2 * k + 1].wait()
        put(outs[k], order, dot(grads[0], gate_ref[k], NT) + dot(grads[1], up_ref[k], NT), parts)


def other_back_kernel(me_ref, dgate_ref, dup_ref, gate_hbm, up_hbm, *refs, parts, orders):
    outs, (gate_ref, up_ref, sems) = refs[: len(orders)], refs[len(orders) :]
    cols = gate_ref.shape[1]
    late = []
    for k, (mask, _) in enumerate(orders):
        first = pl.multiple_of((me_ref[0] ^ mask) * cols, cols)
        late.append(pltpu.make_async_copy(gate_hbm.at[pl.ds(first, cols)], gate_ref.at[k], sems.at[2 * k]))
        late.append(pltpu.make_async_copy(up_hbm.at[pl.ds(first, cols)], up_ref.at[k], sems.at[2 * k + 1]))
    for copy in late:
        copy.start()
    grads = [ref[...].reshape(-1, ref.shape[2]) for ref in (dgate_ref, dup_ref)]
    for k, (_, order) in enumerate(orders):
        late[2 * k].wait()
        late[2 * k + 1].wait()
        put(outs[k], order, dot(grads[0], gate_ref[k], NT) + dot(grads[1], up_ref[k], NT), parts)


def head(h):
    return slice(h * DK, (h + 1) * DK)


def local_kernel(me_ref, rates_ref, query_ref, cot_ref, mixer_hbm, out_hbm, states, sems, *, heads, half):
    dests, _, _ = out_hbm.shape
    tokens = query_ref.shape[0]
    packed = states.shape[0]
    mine = (me_ref[0] % 2) * half
    copies = []
    for s in range(dests):
        first = pl.multiple_of(s * 2 * half + mine, half)
        copies.append(
            pltpu.make_async_copy(
                mixer_hbm.at[:, pl.ds(first, half)], out_hbm.at[s, pl.ds(packed, tokens), :], sems.at[s]
            )
        )
    for copy in copies:
        copy.start()
    row = lax.broadcasted_iota(jnp.int32, (tokens, DK), 0).astype(F32)
    for h in range(heads):
        lead = jnp.exp(-rates_ref[h] * (row + 1.0))
        decayed = (query_ref[:, head(h)].astype(F32) * lead).astype(BF16)
        state = dot(decayed, cot_ref[:, head(h)], TN)
        states[(h // 2) * DK : (h // 2 + 1) * DK, head(h % 2)] = state.astype(BF16)
    sends = [
        pltpu.make_async_copy(states, out_hbm.at[s, pl.ds(0, packed), :], sems.at[dests + s]) for s in range(dests)
    ]
    for copy in sends:
        copy.start()
    for copy in copies + sends:
        copy.wait()


def inner_kernel(rates_ref, query_ref, key_ref, value_ref, cot_ref, entry_ref, gq_ref, gk_ref, gv_ref, *, heads):
    tokens = query_ref.shape[0]
    scale = DK ** (-0.5)
    gap = (
        lax.broadcasted_iota(jnp.int32, (tokens, tokens), 0) - lax.broadcasted_iota(jnp.int32, (tokens, tokens), 1)
    ).astype(F32)
    row = lax.broadcasted_iota(jnp.int32, (tokens, DK), 0).astype(F32)
    for h in range(heads):
        rate = rates_ref[h]
        decay = jnp.where(gap >= 0.0, jnp.exp(-rate * jnp.maximum(gap, 0.0)), 0.0)
        query, key, value, cot = (ref[:, head(h)] for ref in (query_ref, key_ref, value_ref, cot_ref))
        fwd = (dot(query, key, NT) * scale * decay).astype(BF16)
        bwd = (dot(cot, value, NT) * decay).astype(BF16)
        lead = jnp.exp(-rate * (row + 1.0))
        gq = scale * dot(bwd, key) + lead * dot(cot, entry_ref[0, h].astype(BF16), NT)
        gq_ref[:, head(h)] = gq.astype(BF16)
        gk_ref[:, head(h)] = scale * dot(bwd, query, TN)
        gv_ref[:, head(h)] = dot(fwd, cot, TN)


def final_kernel(here_ref, rates_ref, key_ref, value_ref, gk_part, gv_part, got_hbm, gk_ref, gv_ref, states, sem, *, heads):
    devices, packed, lanes = states.shape
    copy = pltpu.make_async_copy(got_hbm.at[:, pl.ds(0, packed), :], states, sem)
    copy.start()
    tokens = key_ref.shape[0]
    scale = DK ** (-0.5)
    lane = lax.broadcasted_iota(jnp.int32, (1, lanes), 1)
    row = lax.broadcasted_iota(jnp.int32, (tokens, DK), 0).astype(F32)
    copy.wait()
    for g in range(heads // 2):
        rate = jnp.where(lane < DK, rates_ref[2 * g], rates_ref[2 * g + 1])

        def add(s, total):
            ahead = s - here_ref[0]
            far = (tokens * jnp.maximum(ahead - 1, 0)).astype(F32)
            step = jnp.where(ahead > 0, jnp.exp(-rate * far), 0.0)
            return total + step * states[s, g * DK : (g + 1) * DK, :].astype(F32)

        reverse = lax.fori_loop(0, devices, add, jnp.zeros((DK, lanes), F32), unroll=devices <= 8).astype(BF16)
        for q in range(2):
            h = 2 * g + q
            tail = scale * jnp.exp(-rates_ref[h] * (tokens - 1.0 - row))
            state = reverse[:, head(q)]
            gk_ref[:, head(h)] = (gk_part[:, head(h)] + tail * dot(value_ref[:, head(h)], state, NT)).astype(BF16)
            gv_ref[:, head(h)] = (gv_part[:, head(h)] + tail * dot(key_ref[:, head(h)], state)).astype(BF16)


def proj_kernel(me_ref, mine_hbm, other_ref, mixed_ref, out_ref, mine_ref, sem):
    devices, tokens, half = mine_ref.shape
    copy = pltpu.make_async_copy(mine_hbm.at[:, pl.ds(mine_hbm.shape[1] - tokens, tokens), :], mine_ref, sem)
    copy.start()
    mixed = mixed_ref[...].reshape(devices * tokens, -1)
    side = me_ref[0] % 2
    out_ref[pl.ds(pl.multiple_of((1 - side) * half, half), half), :] = dot(
        other_ref[...].reshape(devices * tokens, half), mixed, TN
    )
    copy.wait()
    out_ref[pl.ds(pl.multiple_of(side * half, half), half), :] = dot(
        mine_ref[...].reshape(devices * tokens, half), mixed, TN
    )


def vmem():
    return pl.BlockSpec(memory_space=pltpu.VMEM)


def smem():
    return pl.BlockSpec(memory_space=pltpu.SMEM)


def anywhere():
    return pl.BlockSpec(memory_space=pl.ANY)


def sds(shape, dtype):
    return jax.ShapeDtypeStruct(tuple(shape), dtype)


def cost(flops, nbytes):
    return pl.CostEstimate(flops=int(flops), bytes_accessed=int(nbytes), transcendentals=0)


def per_device(
    layer_input,
    out_cot,
    routes,
    route_weights,
    gate_weights,
    up_weights,
    down_weights,
    out_proj,
    queries,
    keys,
    values,
    mixer_out,
    entry_states,
):
    tok_rows, width = layer_input.shape
    experts = lax.axis_size("sp")
    narrow = lax.axis_size("tp")
    here = lax.axis_index("sp")
    me = lax.axis_index("tp")
    me_arr = me.astype(jnp.int32).reshape(1)
    here_arr = here.astype(jnp.int32).reshape(1)
    capacity = 2 * tok_rows * routes.shape[1] // experts
    share = capacity // narrow
    picks = experts * share
    cols = width // narrow
    gate_w, up_w, down_w = gate_weights[0], up_weights[0], down_weights[0]
    hidden = gate_w.shape[1]
    bits = [1 << b for b in range(narrow.bit_length() - 1)]
    routes_t = routes.T
    sems = pltpu.SemaphoreType.DMA

    def swap(value, mask):
        return lax.ppermute(value, "tp", [(i, i ^ mask) for i in range(narrow)])

    def exchange(value):
        return lax.all_to_all(value, "sp", split_axis=0, concat_axis=0, tiled=True)

    part_rows, part_cot = pl.pallas_call(
        functools.partial(dispatch_kernel, experts=experts, share=share),
        out_shape=[sds((picks, width), BF16)] * 2,
        in_specs=[smem(), vmem(), vmem(), anywhere(), anywhere()],
        out_specs=[vmem(), vmem()],
        scratch_shapes=[pltpu.VMEM((tok_rows, width), BF16)] * 2 + [sems((2,))],
        name="dispatch",
    )(me_arr, routes_t, route_weights.T, layer_input, out_cot)
    got_rows = exchange(part_rows.reshape(experts, share, width)).reshape(picks, width)
    got_cot = exchange(part_cot.reshape(experts, share, width)).reshape(picks, width)

    def spread_over_tp(value):
        found = [value]
        for bit in reversed(bits):
            found = found + [swap(v, bit) for v in found]
        return found

    masks = [0]
    for bit in reversed(bits):
        masks = masks + [m | bit for m in masks]
    rows = spread_over_tp(got_rows)
    cots = spread_over_tp(got_cot)

    act, fac_gate, fac_up = pl.pallas_call(
        functools.partial(hidden_kernel, parts=narrow),
        out_shape=[
            sds((narrow, picks, hidden), BF16),
            sds((narrow, picks, hidden), F32),
            sds((narrow, picks, hidden), F32),
        ],
        in_specs=[anywhere()] * (narrow + 2),
        out_specs=[vmem()] * 3,
        scratch_shapes=[pltpu.VMEM((narrow, picks, width), BF16)]
        + [pltpu.VMEM((width, hidden), BF16)] * 2
        + [sems((narrow + 2,))],
        cost_estimate=cost(4 * narrow * picks * width * hidden, 6e6),
        name="hidden",
    )(*rows, gate_w, up_w)

    mixed, _ = lax.optimization_barrier((mixer_out, got_cot))
    mixed_all = exchange(jnp.broadcast_to(mixed[None], (experts, *mixed.shape)))

    position = {m: p for p, m in enumerate(masks)}
    orders = [(m, [position[masks[p] ^ m] for p in range(narrow)]) for m in range(narrow)]
    blocks = (experts, narrow, share, cols) if share % 16 == 0 else (narrow, picks, cols)
    half_count = narrow // 2
    early = [orders[m] for m in reversed(range(half_count, narrow))]
    later = [orders[m] for m in reversed(range(half_count))]
    back = pl.pallas_call(
        functools.partial(first_back_kernel, parts=narrow, orders=early),
        out_shape=[sds((narrow, picks, hidden), BF16)] * 2 + [sds(blocks, BF16)] * len(early),
        in_specs=[smem()] + [anywhere()] * (narrow + 5),
        out_specs=[vmem()] * (2 + len(early)),
        scratch_shapes=[
            pltpu.VMEM((narrow * picks, width), BF16),
            pltpu.VMEM((hidden, width), BF16),
            pltpu.VMEM((narrow, picks, hidden), F32),
            pltpu.VMEM((narrow, picks, hidden), F32),
            pltpu.VMEM((len(early), cols, hidden), BF16),
            pltpu.VMEM((len(early), cols, hidden), BF16),
            sems((narrow + 3 + 2 * len(early),)),
        ],
        cost_estimate=cost(4 * narrow * picks * width * hidden, 9e6),
        name="back",
    )(me_arr, *cots, down_w, fac_gate, fac_up, gate_w, up_w)
    d_gate, d_up = back[:2]
    rest = pl.pallas_call(
        functools.partial(other_back_kernel, parts=narrow, orders=later),
        out_shape=[sds(blocks, BF16)] * len(later),
        in_specs=[smem(), vmem(), vmem(), anywhere(), anywhere()],
        out_specs=[vmem()] * len(later),
        scratch_shapes=[pltpu.VMEM((len(later), cols, hidden), BF16)] * 2 + [sems((2 * len(later),))],
        cost_estimate=cost(2 * narrow * picks * width * hidden, 4e6),
        name="back_rest",
    )(me_arr, d_gate, d_up, gate_w, up_w)
    partial = (list(back[2:]) + list(rest))[::-1]
    for bit in bits:
        for m in reversed(range(0, narrow, 2 * bit)):
            received = swap(partial[m + bit], bit)
            partial[m] = (partial[m].astype(F32) + received.astype(F32)).astype(BF16)
    returning = partial[0]
    if returning.ndim == 3:
        returning = returning.reshape(narrow, experts, share, cols).transpose(1, 0, 2, 3)
    returning, mixed_all = lax.optimization_barrier((returning, mixed_all))
    returned = exchange(returning.reshape(experts, capacity, cols)).reshape(experts * capacity, cols)
    places = pl.pallas_call(
        functools.partial(places_kernel, experts=experts, share=share, masks=masks),
        out_shape=sds((tok_rows, experts * capacity), BF16),
        in_specs=[smem(), vmem()],
        out_specs=vmem(),
        name="places",
    )(me_arr, routes_t)
    own_cols = lax.dynamic_slice_in_dim(out_cot, me * cols, cols, 1)
    cot_cols = (own_cols.astype(F32) + dot(places, returned)).astype(BF16)
    mixer_cot = lax.all_gather(cot_cols, "tp", axis=1, tiled=True)

    all_rows = jnp.concatenate(rows, 0)
    grad_gate = dot(all_rows, d_gate.reshape(-1, hidden), TN).astype(BF16)[None]
    grad_up = dot(all_rows, d_up.reshape(-1, hidden), TN).astype(BF16)[None]
    all_cots = jnp.concatenate(cots, 0)
    grad_down = dot(act.reshape(-1, hidden), all_cots, TN).astype(BF16)[None]

    channels = queries.shape[1]
    heads = channels // DK
    head_ids = (me * heads + jnp.arange(heads, dtype=jnp.int32)).astype(F32)
    rates = decay_rates(head_ids, heads * narrow, tok_rows * experts)
    positions = (here * tok_rows + jnp.arange(tok_rows, dtype=jnp.int32)).astype(F32)
    norm = jnp.repeat(position_norm(positions, rates), DK, axis=1)
    head_cot = (dot(mixer_cot, out_proj) * norm).astype(BF16)
    packed = heads // 2 * DK
    half = width // experts // 2
    flat = (tok_rows, channels)
    if half == 2 * DK:
        sent = pl.pallas_call(
            functools.partial(local_kernel, heads=heads, half=half),
            out_shape=sds((experts, packed + tok_rows, 2 * DK), BF16),
            in_specs=[smem(), smem(), vmem(), vmem(), anywhere()],
            out_specs=anywhere(),
            scratch_shapes=[pltpu.VMEM((packed, 2 * DK), BF16), sems((2 * experts,))],
            name="local",
        )(me_arr, rates, queries, head_cot, mixer_cot)
        got = exchange(sent)
        other = swap(got[:, packed:], 1)
        grad_proj = pl.pallas_call(
            proj_kernel,
            out_shape=sds((2 * half, channels), F32),
            in_specs=[smem(), anywhere(), vmem(), vmem()],
            out_specs=vmem(),
            scratch_shapes=[pltpu.VMEM((experts, tok_rows, half), BF16), sems],
            name="proj",
        )(me_arr, got, other, mixed_all)
    else:
        row = jnp.arange(tok_rows, dtype=F32)[:, None, None]
        lead = jnp.exp(-rates[None, :, None] * (row + 1.0))
        decayed = (queries.reshape(tok_rows, heads, DK).astype(F32) * lead).astype(BF16)
        state = jnp.einsum(
            "ighd,ighe->gdhe",
            decayed.reshape(tok_rows, heads // 2, 2, DK),
            head_cot.reshape(tok_rows, heads // 2, 2, DK),
            preferred_element_type=F32,
        )
        state = state.astype(BF16).reshape(1, packed, 2 * DK)
        got = exchange(jnp.broadcast_to(state, (experts, packed, 2 * DK)))
        slices = lax.all_to_all(mixer_cot, "sp", split_axis=1, concat_axis=0, tiled=True)
        grad_proj = dot(slices, mixed_all.reshape(-1, channels), TN)
    grad_q, gk_part, gv_part = pl.pallas_call(
        functools.partial(inner_kernel, heads=heads),
        out_shape=[sds(flat, BF16), sds(flat, F32), sds(flat, F32)],
        in_specs=[smem()] + [vmem()] * 5,
        out_specs=[vmem()] * 3,
        cost_estimate=cost(heads * 5 * 2 * tok_rows * tok_rows * DK, 2e6),
        name="inner",
    )(rates, queries, keys, values, head_cot, entry_states)
    grad_k, grad_v = pl.pallas_call(
        functools.partial(final_kernel, heads=heads),
        out_shape=[sds(flat, BF16)] * 2,
        in_specs=[smem(), smem()] + [vmem()] * 4 + [anywhere()],
        out_specs=[vmem()] * 2,
        scratch_shapes=[pltpu.VMEM((experts, packed, 2 * DK), BF16), sems],
        name="final",
    )(here_arr, rates, keys, values, gk_part, gv_part, got)
    return grad_gate, grad_up, grad_down, grad_proj, grad_q, grad_k, grad_v


def solution(mesh):
    return jax.shard_map(
        per_device,
        mesh=mesh,
        in_specs=(
            P("sp", None),
            P("sp", None),
            P("sp", None),
            P("sp", None),
            P("sp", None, "tp"),
            P("sp", None, "tp"),
            P("sp", "tp", None),
            P(None, "tp"),
            P("sp", "tp"),
            P("sp", "tp"),
            P("sp", "tp"),
            P("sp", "tp"),
            P("sp", "tp", None, None),
        ),
        out_specs=(
            P("sp", None, "tp"),
            P("sp", None, "tp"),
            P("sp", "tp", None),
            P("sp", "tp"),
            P("sp", "tp"),
            P("sp", "tp"),
            P("sp", "tp"),
        ),
        check_vma=False,
    )
```

time: 196 us -> 175 us (0.89)
  waiting for transfers between devices: 83 us -> 59.1 us
  Pallas kernels: 17.7 us -> 40.3 us
  local copies, waits for them, and re-layouts: 15.9 us -> 3.63 us
  matrix products: 17.1 us -> 12.5 us
  starting transfers between devices: 26.3 us -> 24 us
    pallas_call x2 -> x7, Pallas kernels: 10.2 us -> 32.4 us  [the longest x1 10.2 us: per_device(): pl.pallas_call(functools.partial(local_kernel, heads=heads, half=half), o...]
    all_to_all x4, waiting for transfers between devices: 49.6 us -> 36.1 us  [exchange(): return lax.all_to_all(value, 'sp', split_axis=0, concat_axis=0, tiled=True)]
    unnamed x52 -> x16, local copies, waits for them, and re-layouts: 10.6 us -> 0.74 us
    all_to_all x1 -> x0, waiting for transfers between devices: 8.76 us -> none  [per_device(): lax.all_to_all(mixer_cot, 'sp', split_axis=1, concat_axis=0, tiled=True)]
    dot_general x8 -> x0, matrix products: 5.27 us -> none  [ein(): return jnp.einsum(spec, a, b, preferred_element_type=F32)]
    all_to_all x1 -> x0, starting transfers between devices: 3.57 us -> none  [per_device(): lax.all_to_all(mixer_cot, 'sp', split_axis=1, concat_axis=0, tiled=True)]
    ppermute x9 -> x10, waiting for transfers between devices: 24.7 us -> 23 us  [swap(): return lax.ppermute(value, 'tp', [(i, i ^ mask) for i in range(narrow)])]
    ppermute x9 -> x10, starting transfers between devices: 5.74 us -> 5.93 us  [swap(): return lax.ppermute(value, 'tp', [(i, i ^ mask) for i in range(narrow)])]
  transfers between devices with their start and end apart: 14 -> 14, of which waited for: 8 -> 5; matrix products, arithmetic and copies ran while one was open for 13% -> 10% of each run, Pallas kernels for 2% -> 13%
where the time goes in v2:
time: 175 us; the launch traced here: 174 us
  waiting for transfers between devices  59.1 us (34%)
  Pallas kernels  40.3 us (23%)
  blocking collectives  29.1 us (17%)
  starting transfers between devices  24 us (14%)
  matrix products  12.5 us (7%)
  other arithmetic  4.14 us (2%)
  local copies, waits for them, and re-layouts  3.63 us (2%)
    all_to_all x4, waiting for transfers between devices, exchange(): return lax.all_to_all(value, 'sp', split_axis=0, concat_axis=0, tiled=True)  36.1 us
    ppermute x10, waiting for transfers between devices, swap(): return lax.ppermute(value, 'tp', [(i, i ^ mask) for i in range(narrow)])  23 us
    all_to_all x1, blocking collectives, exchange(): return lax.all_to_all(value, 'sp', split_axis=0, concat_axis=0, tiled=True)  21.9 us
    all_to_all x4, starting transfers between devices, exchange(): return lax.all_to_all(value, 'sp', split_axis=0, concat_axis=0, tiled=True)  18 us
    dot_general x5, matrix products, dot(): lax.dot_general(a, b, dims, precision=precision, preferred_element_type=F32)  12.5 us
    pallas_call x1, Pallas kernels, per_device(): pl.pallas_call(functools.partial(local_kernel, heads=heads, half=half), o...  10.2 us
    all_gather x1, blocking collectives, per_device(): mixer_cot = lax.all_gather(cot_cols, 'tp', axis=1, tiled=True)  7.2 us
    ppermute x10, starting transfers between devices, swap(): return lax.ppermute(value, 'tp', [(i, i ^ mask) for i in range(narrow)])  5.93 us
  transfers between devices with their start and end apart: 14, of which 5 were waited for; matrix products, arithmetic and copies ran while one was open for 10% of the time, Pallas kernels for 13%

profile of v2, /device:TPU:0, one launch (start us, length us, event | category | flops | bytes accessed | tf_op | source)
XLA Modules:
  0.0 173.8 jit_solution(17354829173847903183)
XLA Ops:
  0.7 3.3 %dispatch.1 = (bf16[128,2048]{1,0:T(8,128)(2,1)}, bf16[128,2048]{1,0:T(8,128)(2,1)}) custom-call(s32[1]{0:T(128)} %bitcast.me_ref, s32[2,128]{1,0:T(2,128)} %bitcast.43, f32[2,128]{1,0:T(2,128)} %bitcast.45, bf16[128,2048]{1,0:T(8,128)(2,1)} %rows_hbm.1, bf16[128,2048]{1,0:T(8,128)(2,1)} %cot_hbm.1), custom_call_target="tpu_custom_call" | custom-call | tf_op jit(solution)/shard_map/dispatch/pallas_call | solution.py:335
  4.0 21.9 %all_to_all.25 = bf16[8,16,2048]{2,1,0:T(8,128)(2,1)} all-to-all(bf16[8,16,2048]{2,1,0:T(8,128)(2,1)} %bitcast.40), channel_id=1, replica_groups=mesh['sp'=8,'tp'=4] {'sp'}, dimensions={0} | all-to-all | bytes 1048576 | tf_op jit(solution)/shard_map/all_to_all | solution.py:333
  25.9 4.1 %all-to-all-start.1 = ((bf16[8,16,2048]{2,1,0:T(8,128)(2,1)}), bf16[8,16,2048]{2,1,0:T(8,128)(2,1)}, u32[]{:S(2)}, u32[]{:S(2)}) async-start(bf16[8,16,2048]{2,1,0:T(8,128)(2,1)} %bitcast.39), calls=%async_computation.1 | async-start | bytes 1048576 | tf_op jit(solution)/shard_map/all_to_all | solution.py:333
  31.7 12.1 %all-to-all-done.1 = bf16[8,16,2048]{2,1,0:T(8,128)(2,1)} async-done(((bf16[8,16,2048]{2,1,0:T(8,128)(2,1)}), bf16[8,16,2048]{2,1,0:T(8,128)(2,1)}, u32[]{:S(2)}, u32[]{:S(2)}) %all-to-all-start.1) | async-done | bytes 524320 | tf_op jit(solution)/shard_map/all_to_all | solution.py:333
  45.9 10.5 %collective-permute-done.3.refs_1_ = bf16[128,2048]{1,0:T(8,128)(2,1)} collective-permute-done((bf16[128,2048]{1,0:T(8,128)(2,1)}, bf16[128,2048]{1,0:T(8,128)(2,1)}, u32[]{:S(2)}, u32[]{:S(2)}) %collective-permute-start.3) | collective-permute-done | bytes 524320 | tf_op jit(solution)/shard_map/ppermute | solution.py:330
  57.4 4.4 %all-to-all-start.2 = ((bf16[8,128,512]{2,1,0:T(8,128)(2,1)}), bf16[8,128,512]{2,1,0:T(8,128)(2,1)S(1)}, u32[]{:S(2)}, u32[]{:S(2)}) async-start(bf16[8,128,512]{2,1,0:T(8,128)(2,1)} %broadcast_in_dim.24), calls=%async_computation.2 | async-start | bytes 2097152 | tf_op jit(solution)/shard_map/all_to_all | solution.py:333
  61.8 4.7 %hidden.1 = (bf16[4,128,256]{2,1,0:T(8,128)(2,1)}, f32[4,128,256]{2,1,0:T(8,128)}, f32[4,128,256]{2,1,0:T(8,128)}) custom-call(bf16[128,2048]{1,0:T(8,128)(2,1)} %bitcast.4.refs_0_, bf16[128,2048]{1,0:T(8,128)(2,1)} %collective-permute-done.refs_1_, bf16[128,2048]{1,0:T(8,128)(2,1)} %collective-permute-done.1.refs_2_, ...), custom_call_target="tpu_custom_call" | custom-call | flops 1073741824 | bytes 6000000 | tf_op jit(solution)/shard_map/hidden/pallas_call | solution.py:358
  66.5 5.8 %back.1 = (bf16[4,128,256]{2,1,0:T(8,128)(2,1)}, bf16[4,128,256]{2,1,0:T(8,128)(2,1)}, bf16[8,4,16,512]{3,2,1,0:T(8,128)(2,1)}, bf16[8,4,16,512]{3,2,1,0:T(8,128)(2,1)}) custom-call(s32[1]{0:T(128)} %bitcast.me_ref, bf16[128,2048]{1,0:T(8,128)(2,1)} %bitcast.6.refs_0_, bf16[128,2048]{1,0:T(8,128)(2,1)} %collective-permute-done.3.refs_1_, ...), custom_call_target="tpu_custom_call" | custom-call | flops 1073741824 | bytes 9000000 | tf_op jit(solution)/shard_map/back/pallas_call | solution.py:383
  72.5 3.8 %back_rest.1 = (bf16[8,4,16,512]{3,2,1,0:T(8,128)(2,1)}, bf16[8,4,16,512]{3,2,1,0:T(8,128)(2,1)}) custom-call(s32[1]{0:T(128)} %bitcast.me_ref, bf16[4,128,256]{2,1,0:T(8,128)(2,1)} %get-tuple-element.30.dgate_ref, bf16[4,128,256]{2,1,0:T(8,128)(2,1)} %get-tuple-element.31.dup_ref, bf16[2048,256]{1,0:T(8,128)(2,1)} %bitcast.32, bf16[2048,256]{1,0:T(8,128)(2,1)} %bitcast.35), custom_call_target="tpu_custom_call" | custom-call | flops 536870912 | bytes 4000000 | tf_op jit(solution)/shard_map/back_rest/pallas_call | solution.py:401
  79.7 12.5 %collective-permute-done.8 = bf16[8,4,16,512]{3,2,1,0:T(8,128)(2,1)S(1)} collective-permute-done((bf16[8,4,16,512]{3,2,1,0:T(8,128)(2,1)S(1)}, bf16[8,4,16,512]{3,2,1,0:T(8,128)(2,1)S(1)}, u32[]{:S(2)}, u32[]{:S(2)}) %collective-permute-start.8) | collective-permute-done | bytes 524320 | tf_op jit(solution)/shard_map/ppermute | solution.py:330
  92.2 2.1 %add_convert_fusion = bf16[8,4,16,512]{3,2,1,0:T(8,128)(2,1)} fusion(bf16[8,4,16,512]{3,2,1,0:T(8,128)(2,1)S(1)} %collective-permute-done.8, bf16[8,4,16,512]{3,2,1,0:T(8,128)(2,1)S(1)} %collective-permute-done.6, bf16[8,4,16,512]{3,2,1,0:T(8,128)(2,1)} %get-tuple-element.33), kind=kLoop, calls=%fused_computation.18 | loop fusion | flops 2097152 | bytes 2097152 | tf_op jit(solution)/shard_map/convert_element_type | solution.py:414
  94.3 5.8 %all-to-all-start.3 = ((bf16[8,64,512]{2,1,0:T(8,128)(2,1)}), bf16[8,64,512]{2,1,0:T(8,128)(2,1)}, u32[]{:S(2)}, u32[]{:S(2)}) async-start(bf16[8,64,512]{2,1,0:T(8,128)(2,1)} %bitcast.36), calls=%async_computation.3 | async-start | bytes 1048576 | tf_op jit(solution)/shard_map/all_to_all | solution.py:333
  100.1 1.7 places.1
  104.3 9.8 %all-to-all-done.3 = bf16[8,64,512]{2,1,0:T(8,128)(2,1)} async-done(((bf16[8,64,512]{2,1,0:T(8,128)(2,1)}), bf16[8,64,512]{2,1,0:T(8,128)(2,1)}, u32[]{:S(2)}, u32[]{:S(2)}) %all-to-all-start.3) | async-done | bytes 524320 | tf_op jit(solution)/shard_map/all_to_all | solution.py:333
  115.4 7.2 %all_gather.3.mixer_hbm = bf16[128,2048]{1,0:T(8,128)(2,1)S(1)} all-gather(bf16[128,512]{1,0:T(8,128)(2,1)S(1)} %fusion.10), channel_id=1, replica_groups=mesh['sp'=8,'tp'=4] {'tp'}, dimensions={1}, use_global_device_ids=true | all-gather | bytes 655360 | tf_op jit(solution)/shard_map/all_gather | solution.py:429
  123.8 10.2 %local.1 = bf16[8,384,128]{2,1,0:T(8,128)(2,1)} custom-call(s32[1]{0:T(128)} %bitcast.me_ref, f32[8]{0:T(128)} %get-tuple-element.45.rates_ref, bf16[128,512]{1,0:T(8,128)(2,1)} %query_ref.3, bf16[128,512]{1,0:T(8,128)(2,1)} %fusion.11.cot_ref, bf16[128,2048]{1,0:T(8,128)(2,1)} %copy-done.2), custom_call_target="tpu_custom_call" | custom-call | tf_op jit(solution)/shard_map/local/pallas_call | solution.py:448
  134.0 3.7 %all-to-all-start.4 = ((bf16[8,384,128]{2,1,0:T(8,128)(2,1)}), bf16[8,384,128]{2,1,0:T(8,128)(2,1)S(1)}, u32[]{:S(2)}, u32[]{:S(2)}) async-start(bf16[8,384,128]{2,1,0:T(8,128)(2,1)} %local.1), calls=%async_computation.4 | async-start | bytes 1572864 | tf_op jit(solution)/shard_map/all_to_all | solution.py:333
  137.8 3.3 %fusion.1 = bf16[1,2048,256]{2,1,0:T(8,128)(2,1)} fusion(bf16[512,256]{1,0:T(8,128)(2,1)S(1)} %bitcast.42, bf16[128,2048]{1,0:T(8,128)(2,1)} %collective-permute-done.2.refs_3_, bf16[128,2048]{1,0:T(8,128)(2,1)} %collective-permute-done.1.refs_2_, bf16[128,2048]{1,0:T(8,128)(2,1)} %collective-permute-done.refs_1_, bf16[128,2048]{1,0:T(8,128)(2,1)} %bitcast.4.refs_0_), kind=kOutput, calls=%fused_computation.4 | convolution fusion | flops 545783808 | bytes 3407872 | tf_op jit(solution)/shard_map/dot_general | solution.py:20
  141.1 3.3 %fusion = bf16[1,2048,256]{2,1,0:T(8,128)(2,1)} fusion(bf16[512,256]{1,0:T(8,128)(2,1)S(1)} %bitcast.41, bf16[128,2048]{1,0:T(8,128)(2,1)} %collective-permute-done.2.refs_3_, bf16[128,2048]{1,0:T(8,128)(2,1)} %collective-permute-done.1.refs_2_, bf16[128,2048]{1,0:T(8,128)(2,1)} %collective-permute-done.refs_1_, bf16[128,2048]{1,0:T(8,128)(2,1)} %bitcast.4.refs_0_), kind=kOutput, calls=%fused_computation.3 | convolution fusion | flops 545783808 | bytes 3407872 | tf_op jit(solution)/shard_map/dot_general | solution.py:20
  144.3 14.1 %all-to-all-done.4.mine_hbm.got_hbm = bf16[8,384,128]{2,1,0:T(8,128)(2,1)S(1)} async-done(((bf16[8,384,128]{2,1,0:T(8,128)(2,1)}), bf16[8,384,128]{2,1,0:T(8,128)(2,1)S(1)}, u32[]{:S(2)}, u32[]{:S(2)}) %all-to-all-start.4) | async-done | bytes 786464 | tf_op jit(solution)/shard_map/all_to_all | solution.py:333
  158.5 3.5 %fusion.2 = bf16[1,256,2048]{2,1,0:T(8,128)(2,1)} fusion(bf16[512,256]{1,0:T(8,128)(2,1)} %bitcast.46, bf16[128,2048]{1,0:T(8,128)(2,1)} %collective-permute-done.5.refs_3_, bf16[128,2048]{1,0:T(8,128)(2,1)} %collective-permute-done.4.refs_2_, bf16[128,2048]{1,0:T(8,128)(2,1)} %collective-permute-done.3.refs_1_, bf16[128,2048]{1,0:T(8,128)(2,1)} %bitcast.6.refs_0_), kind=kOutput, calls=%fused_computation.5 | convolution fusion | flops 545783808 | bytes 3407872 | tf_op jit(solution)/shard_map/dot_general | solution.py:20
  162.0 4.1 %inner.1 = (bf16[128,512]{1,0:T(8,128)(2,1)}, f32[128,512]{1,0:T(8,128)}, f32[128,512]{1,0:T(8,128)}) custom-call(f32[8]{0:T(128)} %get-tuple-element.45.rates_ref, bf16[128,512]{1,0:T(8,128)(2,1)} %query_ref.3, bf16[128,512]{1,0:T(8,128)(2,1)} %key_ref.3, bf16[128,512]{1,0:T(8,128)(2,1)} %value_ref.3, bf16[128,512]{1,0:T(8,128)(2,1)} %fusion.11.cot_ref, ...), custom_call_target="tpu_custom_call" | custom-call | flops 83886080 | bytes 2000000 | tf_op jit(solution)/shard_map/inner/pallas_call | solution.py:480
  166.1 3.4 %final.1 = (bf16[128,512]{1,0:T(8,128)(2,1)}, bf16[128,512]{1,0:T(8,128)(2,1)}) custom-call(s32[1]{0:T(128)} %bitcast.19.here_ref, f32[8]{0:T(128)} %get-tuple-element.45.rates_ref, bf16[128,512]{1,0:T(8,128)(2,1)} %key_ref.3, bf16[128,512]{1,0:T(8,128)(2,1)} %value_ref.3, f32[128,512]{1,0:T(8,128)} %get-tuple-element.41.gk_part, ...), custom_call_target="tpu_custom_call" | custom-call | tf_op jit(solution)/shard_map/final/pallas_call | solution.py:488
  170.2 3.4 %proj.1 = f32[256,512]{1,0:T(8,128)} custom-call(s32[1]{0:T(128)} %bitcast.me_ref, bf16[8,384,128]{2,1,0:T(8,128)(2,1)} %copy-done.1, bf16[8,128,128]{2,1,0:T(8,128)(2,1)} %copy-done.6, bf16[8,128,512]{2,1,0:T(8,128)(2,1)} %copy-done.3), custom_call_target="tpu_custom_call" | custom-call | tf_op jit(solution)/shard_map/proj/pallas_call | solution.py:458
  (46 shorter events, 14.1 us)
Async XLA Ops:
  0.6 122.0 %copy-start = (bf16[2048,512]{1,0:T(8,128)(2,1)S(1)}, bf16[2048,512]{1,0:T(8,128)(2,1)}, u32[]{:S(2)}) copy-start(bf16[2048,512]{1,0:T(8,128)(2,1)} %param.20) | copy-start | bytes 6291460
  0.6 55.7 %copy-start.7 = (bf16[128,512]{1,0:T(8,128)(2,1)S(1)}, bf16[128,512]{1,0:T(8,128)(2,1)}, u32[]{:S(2)}) copy-start(bf16[128,512]{1,0:T(8,128)(2,1)} %param.24) | copy-start | bytes 393220
  25.9 17.9 %all-to-all-start.1 = ((bf16[8,16,2048]{2,1,0:T(8,128)(2,1)}), bf16[8,16,2048]{2,1,0:T(8,128)(2,1)}, u32[]{:S(2)}, u32[]{:S(2)}) async-start(bf16[8,16,2048]{2,1,0:T(8,128)(2,1)} %bitcast.39), calls=%async_computation.1 | async-start | bytes 1048576 | tf_op jit(solution)/shard_map/all_to_all | solution.py:333
  30.1 15.3 %collective-permute-start = (bf16[128,2048]{1,0:T(8,128)(2,1)}, bf16[128,2048]{1,0:T(8,128)(2,1)}, u32[]{:S(2)}, u32[]{:S(2)}) collective-permute-start(bf16[128,2048]{1,0:T(8,128)(2,1)} %bitcast.4.refs_0_), channel_id=1, source_target_pairs={{0,2},{1,3},{2,0},{3,1},{4,6},{5,7},{6,4},{7,5},{8,10},{9,11},{10,... | collective-permute-start | bytes 1572872 | tf_op jit(solution)/shard_map/ppermute | solution.py:330
  43.8 12.5 %collective-permute-start.3 = (bf16[128,2048]{1,0:T(8,128)(2,1)}, bf16[128,2048]{1,0:T(8,128)(2,1)}, u32[]{:S(2)}, u32[]{:S(2)}) collective-permute-start(bf16[128,2048]{1,0:T(8,128)(2,1)} %bitcast.6.refs_0_), channel_id=1, source_target_pairs={{0,2},{1,3},{2,0},{3,1},{4,6},{5,7},{6,4},{7,5},{8,10},{9,11},{10,... | collective-permute-start | bytes 1572872 | tf_op jit(solution)/shard_map/ppermute | solution.py:330
  45.3 16.4 %collective-permute-start.1 = (bf16[128,2048]{1,0:T(8,128)(2,1)}, bf16[128,2048]{1,0:T(8,128)(2,1)}, u32[]{:S(2)}, u32[]{:S(2)}) collective-permute-start(bf16[128,2048]{1,0:T(8,128)(2,1)} %bitcast.4.refs_0_), channel_id=1, source_target_pairs={{0,1},{1,0},{2,3},{3,2},{4,5},{5,4},{6,7},{7,6},{8,9},{9,8},{10,11... | collective-permute-start | bytes 1572872 | tf_op jit(solution)/shard_map/ppermute | solution.py:330
  45.3 16.4 %collective-permute-start.2 = (bf16[128,2048]{1,0:T(8,128)(2,1)}, bf16[128,2048]{1,0:T(8,128)(2,1)}, u32[]{:S(2)}, u32[]{:S(2)}) collective-permute-start(bf16[128,2048]{1,0:T(8,128)(2,1)} %collective-permute-done.refs_1_), channel_id=1, source_target_pairs={{0,1},{1,0},{2,3},{3,2},{4,5},{5,4},{6,7},{7,6},{8,9},{9,8},{10,11... | collective-permute-start | bytes 1572872 | tf_op jit(solution)/shard_map/ppermute | solution.py:330
  45.9 20.6 %collective-permute-start.4 = (bf16[128,2048]{1,0:T(8,128)(2,1)}, bf16[128,2048]{1,0:T(8,128)(2,1)}, u32[]{:S(2)}, u32[]{:S(2)}) collective-permute-start(bf16[128,2048]{1,0:T(8,128)(2,1)} %bitcast.6.refs_0_), channel_id=1, source_target_pairs={{0,1},{1,0},{2,3},{3,2},{4,5},{5,4},{6,7},{7,6},{8,9},{9,8},{10,11... | collective-permute-start | bytes 1572872 | tf_op jit(solution)/shard_map/ppermute | solution.py:330
  56.3 10.1 %collective-permute-start.5 = (bf16[128,2048]{1,0:T(8,128)(2,1)}, bf16[128,2048]{1,0:T(8,128)(2,1)}, u32[]{:S(2)}, u32[]{:S(2)}) collective-permute-start(bf16[128,2048]{1,0:T(8,128)(2,1)} %collective-permute-done.3.refs_1_), channel_id=1, source_target_pairs={{0,1},{1,0},{2,3},{3,2},{4,5},{5,4},{6,7},{7,6},{8,9},{9,8},{10,11... | collective-permute-start | bytes 1572872 | tf_op jit(solution)/shard_map/ppermute | solution.py:330
  57.4 36.9 %all-to-all-start.2 = ((bf16[8,128,512]{2,1,0:T(8,128)(2,1)}), bf16[8,128,512]{2,1,0:T(8,128)(2,1)S(1)}, u32[]{:S(2)}, u32[]{:S(2)}) async-start(bf16[8,128,512]{2,1,0:T(8,128)(2,1)} %broadcast_in_dim.24), calls=%async_computation.2 | async-start | bytes 2097152 | tf_op jit(solution)/shard_map/all_to_all | solution.py:333
  72.2 4.5 %collective-permute-start.7 = (bf16[8,4,16,512]{3,2,1,0:T(8,128)(2,1)}, bf16[8,4,16,512]{3,2,1,0:T(8,128)(2,1)}, u32[]{:S(2)}, u32[]{:S(2)}) collective-permute-start(bf16[8,4,16,512]{3,2,1,0:T(8,128)(2,1)} %get-tuple-element.36), channel_id=1, source_target_pairs={{0,1},{1,0},{2,3},{3,2},{4,5},{5,4},{6,7},{7,6},{8,9},{9,8},{10,11... | collective-permute-start | bytes 1572872 | tf_op jit(solution)/shard_map/ppermute | solution.py:330
  76.4 3.3 %collective-permute-start.6 = (bf16[8,4,16,512]{3,2,1,0:T(8,128)(2,1)}, bf16[8,4,16,512]{3,2,1,0:T(8,128)(2,1)S(1)}, u32[]{:S(2)}, u32[]{:S(2)}) collective-permute-start(bf16[8,4,16,512]{3,2,1,0:T(8,128)(2,1)} %get-tuple-element.34), channel_id=1, source_target_pairs={{0,1},{1,0},{2,3},{3,2},{4,5},{5,4},{6,7},{7,6},{8,9},{9,8},{10,11... | collective-permute-start | bytes 1572872 | tf_op jit(solution)/shard_map/ppermute | solution.py:330
  78.1 14.1 %collective-permute-start.8 = (bf16[8,4,16,512]{3,2,1,0:T(8,128)(2,1)S(1)}, bf16[8,4,16,512]{3,2,1,0:T(8,128)(2,1)S(1)}, u32[]{:S(2)}, u32[]{:S(2)}) collective-permute-start(bf16[8,4,16,512]{3,2,1,0:T(8,128)(2,1)S(1)} %add_convert_fusion.1), channel_id=1, source_target_pairs={{0,2},{1,3},{2,0},{3,1},{4,6},{5,7},{6,4},{7,5},{8,10},{9,11},{10,... | collective-permute-start | bytes 1572872 | tf_op jit(solution)/shard_map/ppermute | solution.py:330
  94.3 19.8 %copy-start.3 = (bf16[8,128,512]{2,1,0:T(8,128)(2,1)}, bf16[8,128,512]{2,1,0:T(8,128)(2,1)S(1)}, u32[]{:S(2)}) copy-start(bf16[8,128,512]{2,1,0:T(8,128)(2,1)S(1)} %all-to-all-done.2.mixed_ref) | copy-start | bytes 3145732
  94.3 19.8 %all-to-all-start.3 = ((bf16[8,64,512]{2,1,0:T(8,128)(2,1)}), bf16[8,64,512]{2,1,0:T(8,128)(2,1)}, u32[]{:S(2)}, u32[]{:S(2)}) async-start(bf16[8,64,512]{2,1,0:T(8,128)(2,1)} %bitcast.36), calls=%async_computation.3 | async-start | bytes 1048576 | tf_op jit(solution)/shard_map/all_to_all | solution.py:333
  122.6 1.1 copy-start.2
  123.8 14.0 %copy-start.5 = (bf16[4,128,256]{2,1,0:T(8,128)(2,1)S(1)}, bf16[4,128,256]{2,1,0:T(8,128)(2,1)}, u32[]{:S(2)}) copy-start(bf16[4,128,256]{2,1,0:T(8,128)(2,1)} %get-tuple-element.31.dup_ref) | copy-start | bytes 786436
  134.0 24.4 %all-to-all-start.4 = ((bf16[8,384,128]{2,1,0:T(8,128)(2,1)}), bf16[8,384,128]{2,1,0:T(8,128)(2,1)S(1)}, u32[]{:S(2)}, u32[]{:S(2)}) async-start(bf16[8,384,128]{2,1,0:T(8,128)(2,1)} %local.1), calls=%async_computation.4 | async-start | bytes 1572864 | tf_op jit(solution)/shard_map/all_to_all | solution.py:333
  137.8 3.3 %copy-start.4 = (bf16[4,128,256]{2,1,0:T(8,128)(2,1)S(1)}, bf16[4,128,256]{2,1,0:T(8,128)(2,1)}, u32[]{:S(2)}) copy-start(bf16[4,128,256]{2,1,0:T(8,128)(2,1)} %get-tuple-element.30.dgate_ref) | copy-start | bytes 786436
  158.4 3.6 %copy-start.1 = (bf16[8,384,128]{2,1,0:T(8,128)(2,1)}, bf16[8,384,128]{2,1,0:T(8,128)(2,1)S(1)}, u32[]{:S(2)}) copy-start(bf16[8,384,128]{2,1,0:T(8,128)(2,1)S(1)} %all-to-all-done.4.mine_hbm.got_hbm) | copy-start | bytes 2359300
  158.4 11.0 %collective-permute-start.9 = (bf16[8,128,128]{2,1,0:T(8,128)(2,1)S(1)}, bf16[8,128,128]{2,1,0:T(8,128)(2,1)S(1)}, u32[]{:S(2)}, u32[]{:S(2)}) collective-permute-start(bf16[8,128,128]{2,1,0:T(8,128)(2,1)S(1)} %slice.4), channel_id=1, source_target_pairs={{0,1},{1,0},{2,3},{3,2},{4,5},{5,4},{6,7},{7,6},{8,9},{9,8},{10,11... | collective-permute-start | bytes 786440 | tf_op jit(solution)/shard_map/ppermute | solution.py:330
  169.5 0.7 copy-start.6
